TPU v7x, 256 devices: a whole 4x4x8 slice. The times are simulated.
256 devices in a mesh: sp: 64 (over z, x, core), tp: 4 (over y).
Axes of the slice: x: 4, y: 4, z: 8, core: 2. Of those that a mesh axis runs over, the one named last changes fastest.
Arguments:
- residual: bfloat16 [16384, 2048], P(('sp', 'tp')), may hold values from -6 to 6
- queries: bfloat16 [16384, 1024], P('sp', 'tp'), may hold values from -8 to 8
- key_pairs: bfloat16 [16384, 512], P('sp', 'tp'), may hold values from -8 to 8
- values: bfloat16 [16384, 512], P('sp', 'tp'), may hold values from -6 to 6
- lambdas: float32 [8], P('tp'), may hold values from 0.3 to 0.8
- head_gain: float32 [128], replicated, may hold values from 0.1 to 1.9
- out_weight: bfloat16 [1024, 2048], replicated, may hold values from -0.1875 to 0.1875
- mixer_gain: float32 [2048], replicated, may hold values from 0.1 to 1.9
- before_gain: float32 [2048], replicated, may hold values from 0.1 to 1.9
- after_gain: float32 [2048], replicated, may hold values from 0.1 to 1.9
- gate_weight: bfloat16 [2048, 5632], P('sp', 'tp'), may hold values from -0.125 to 0.125
- up_weight: bfloat16 [2048, 5632], P('sp', 'tp'), may hold values from -0.125 to 0.125
- down_weight: bfloat16 [5632, 2048], P('tp', 'sp'), may hold values from -0.078125 to 0.078125
Outputs:
- updated: bfloat16 [16384, 2048], P(('sp', 'tp'))
All inputs are finite; a program needn't handle non-finite values.
Results may differ from a plain program's by a relative error of at most 0.014.
Values may be sent and summed in bfloat16 or wider, within the bound.
No kernel may reach another device: no remote copies, remote signals or barrier semaphores. Data moves between devices by JAX's collectives and lax.ppermute only.
A program may use at most 128 MiB of HBM per device.

v0:
```python
import functools
import math

import jax
import jax.numpy as jnp
from jax import lax
from jax.experimental import pallas as pl
from jax.experimental.pallas import tpu as pltpu
from jax.sharding import Mesh
from jax.sharding import PartitionSpec as P

HEAD_DIM = 64
WIDTH = 2 * HEAD_DIM
Z, X, C, T = "sp_0", "sp_1", "sp_2", "tp"
SP = (Z, X, C)
SP_TP = (Z, X, C, T)
F32, BF16 = jnp.float32, jnp.bfloat16
LOG2E = 1.4426950408889634
VMEM = pl.BlockSpec(memory_space=pltpu.VMEM)
SMEM = pl.BlockSpec(memory_space=pltpu.SMEM)
HBM = pl.BlockSpec(memory_space=pltpu.HBM)
STATE = WIDTH + 8
COLS = 256
PIECE = 256
TILES = 2
TALL = WIDTH + 16
FACTOR = LOG2E / math.sqrt(HEAD_DIM)
LIMIT = 2.0**80


def shifted(array, axis, by):
    count = lax.axis_size(axis)
    return lax.ppermute(array, axis, [((i + by) % count, i) for i in range(count)])


def attend_kernel(first, count, groups, *refs):
    if first:
        queries, kvs, refs = refs[:2], refs[2 : 2 + count], refs[2 + count :]
        ins, (out_a, out_b, tables, keys2, values1) = None, refs
    else:
        kvs, ins, tables, refs = refs[:count], refs[count : count + 2], refs[count + 2], refs[count + 3 :]
        out_a, out_b, keys2, values1 = refs
    outs = (out_a, out_b)
    length = values1.shape[1]
    lane = lax.broadcasted_iota(jnp.int32, (1, WIDTH), 1)
    values1[WIDTH:, :] = jnp.ones((TALL - WIDTH, length), BF16)
    at = 0
    for kv in kvs:
        span = pl.ds(at, kv.shape[0])
        keys = kv[:, :WIDTH]
        for which in range(2):
            keys2[which, span, :WIDTH] = keys
            keys2[which, span, WIDTH:] = jnp.where((lane < HEAD_DIM) == (which == 0), keys, jnp.ones_like(keys))
        values1[:WIDTH, span] = kv[:, WIDTH:].T
        at += kv.shape[0]
    row = lax.broadcasted_iota(jnp.int32, (WIDTH, COLS), 0)
    if first:

        def one_table(group, carry):
            rows = pl.ds(pl.multiple_of(group * COLS, COLS), COLS)
            for half in range(2):
                for head in range(2):
                    query = queries[half][rows, head * WIDTH : (head + 1) * WIDTH].astype(F32).T * FACTOR
                    high = query.astype(BF16).astype(F32)
                    low = query - high
                    for which in range(2):
                        own = (row < HEAD_DIM) == (which == 0)
                        tile = group * 4 + which * 2 + head
                        table = tables.at[half * 4 * groups + tile]
                        lower = jnp.where(own, low, 0.0)
                        table[:WIDTH, :] = jnp.where(own, high, 0.0).astype(BF16)
                        table[WIDTH:, :] = lower.astype(BF16)
                        score = jnp.dot(keys2[which, :COLS, :], table[...], preferred_element_type=F32)
                        top = jnp.max(score, axis=0, keepdims=True).astype(BF16).astype(F32)
                        spot = HEAD_DIM if which == 0 else 0
                        table[WIDTH:, :] = jnp.where(row == spot, -top, lower).astype(BF16)
                        outs[half][tile, WIDTH:, :] = jnp.broadcast_to(top, (8, COLS))
            return carry

        lax.fori_loop(0, groups, one_table, 0)
    line = lax.broadcasted_iota(jnp.int32, (8, COLS), 0)
    piece = length // pl.cdiv(length, PIECE)

    def stats_of(top, total, reference):
        top, reference = jnp.broadcast_to(top, (8, COLS)), jnp.broadcast_to(reference, (8, COLS))
        return jnp.where(line == 0, top, jnp.where(line == 2, reference, total))

    def one_tile(tile, largest):
        which = lax.rem(tile, 4) // 2
        for half in range(2):
            table = tables[half * 4 * groups + tile]
            both = None
            for start in range(0, length, piece):
                score = jnp.dot(keys2[which, start : start + piece, :], table, preferred_element_type=F32)
                expo = jnp.exp2(score).astype(BF16)
                term = jnp.dot(values1[:, start : start + piece], expo, preferred_element_type=F32)
                both = term if both is None else both + term
            numer, total = both[:WIDTH], both[WIDTH:STATE]
            stats = (outs if first else ins)[half][tile, WIDTH:, :]
            top, reference = stats[0:1], stats[2:3]
            if not first:
                numer = numer + ins[half][tile, :WIDTH, :]
                total = total + stats[1:2]
            outs[half][tile, :WIDTH, :] = numer
            outs[half][tile, WIDTH:, :] = stats_of(top, total, reference)
            fine = (total[0:1] < LIMIT) & (top == reference)
            largest = jnp.maximum(largest, jnp.where(fine, 0.0, 1.0))
        return largest

    def some_tiles(i, largest):
        for j in range(TILES):
            largest = one_tile(i * TILES + j, largest)
        return largest

    largest = lax.fori_loop(0, 4 * groups // TILES, some_tiles, jnp.zeros((1, COLS), F32))

    @pl.when(jnp.max(largest) > 0.0)
    def _():
        def redo_tile(tile, carry):
            which = lax.rem(tile, 4) // 2
            for half in range(2):
                table = tables.at[half * 4 * groups + tile]

                def score_of(i):
                    rows = pl.ds(pl.multiple_of(i * COLS, COLS), COLS)
                    return jnp.dot(keys2[which, rows, :], table[...], preferred_element_type=F32), rows

                def find_top(i, top):
                    return jnp.maximum(top, jnp.max(score_of(i)[0], axis=0, keepdims=True))

                above = lax.fori_loop(0, length // COLS, find_top, jnp.zeros((1, COLS), F32))
                stats = (outs if first else ins)[half][tile, WIDTH:, :]
                old_top, reference = stats[0:1], stats[2:3]
                top = jnp.maximum(old_top, reference + above)
                raised = top - reference

                def add(i, both):
                    score, rows = score_of(i)
                    expo = jnp.exp2(score - raised).astype(BF16)
                    cols = pl.ds(pl.multiple_of(i * COLS, COLS), COLS)
                    return both + jnp.dot(values1[:, cols], expo, preferred_element_type=F32)

                both = lax.fori_loop(0, length // COLS, add, jnp.zeros((TALL, COLS), F32))
                numer, total = both[:WIDTH], both[WIDTH:STATE]
                if not first:
                    shrink = jnp.exp2(old_top - top)
                    numer = numer + ins[half][tile, :WIDTH, :] * shrink
                    total = total + stats[1:2] * shrink
                outs[half][tile, :WIDTH, :] = numer
                outs[half][tile, WIDTH:, :] = stats_of(top, total, reference)
            return carry

        lax.fori_loop(0, 4 * groups, redo_tile, 0)


def attend(carried, queries, kvs):
    first = carried is None
    keys = sum(kv.shape[0] for kv in kvs)
    groups = queries[0].shape[0] // COLS
    state = jax.ShapeDtypeStruct((4 * groups, STATE, COLS), F32)
    tables = jax.ShapeDtypeStruct((8 * groups, 2 * WIDTH, COLS), BF16)
    operands = (*queries, *kvs) if first else (*kvs, *carried)
    results = (state, state, tables) if first else (state, state)
    done = pl.pallas_call(
        functools.partial(attend_kernel, first, len(kvs), groups),
        out_shape=results,
        in_specs=[VMEM] * len(operands),
        out_specs=(VMEM,) * len(results),
        scratch_shapes=[pltpu.VMEM((2, keys, 2 * WIDTH), BF16), pltpu.VMEM((TALL, keys), BF16)],
        compiler_params=pltpu.CompilerParams(vmem_limit_bytes=40 << 20),
        cost_estimate=pl.CostEstimate(
            flops=2 * 2048 * groups * keys * 256 * 2,
            bytes_accessed=keys * 512 + (2 << 20),
            transcendentals=2048 * groups * keys,
        ),
        name="attend",
    )(*operands)
    return done if first else (*done, carried[2])


def halves_kernel(mine, theirs, own, *sent):
    line = lax.broadcasted_iota(jnp.int32, (8, COLS), 0)

    def joined(tile):
        a, b = mine.at[tile], theirs.at[tile]
        top_a, top_b = a[WIDTH : WIDTH + 1, :], b[WIDTH : WIDTH + 1, :]
        top = jnp.maximum(top_a, top_b)
        weight_a, weight_b = jnp.exp2(top_a - top), jnp.exp2(top_b - top)
        total = a[WIDTH + 1 : WIDTH + 2, :] * weight_a + b[WIDTH + 1 : WIDTH + 2, :] * weight_b
        return (a[:WIDTH, :] * weight_a + b[:WIDTH, :] * weight_b) / total, top + jnp.log2(total)

    for kind in range(4):
        outcome, level = joined(kind)
        own[kind, :WIDTH, :] = outcome
        own[kind, WIDTH:, :] = jnp.broadcast_to(level, (8, COLS))
        for group, out in enumerate(sent):
            outcome, level = joined(4 * (group + 1) + kind)
            out[kind, :WIDTH, :] = outcome.astype(BF16)
            high = level.astype(BF16).astype(F32)
            middle = (level - high).astype(BF16).astype(F32)
            low = level - high - middle
            parts = jnp.where(line == 0, high, jnp.where(line == 1, middle, low))
            out[kind, WIDTH:, :] = jnp.concatenate((parts, jnp.zeros_like(parts)), axis=0).astype(BF16)


def join_halves(mine, theirs):
    groups = mine.shape[0] // 4
    sent = jax.ShapeDtypeStruct((4, TALL, COLS), BF16)
    return pl.pallas_call(
        halves_kernel,
        out_shape=(jax.ShapeDtypeStruct((4, STATE, COLS), F32),) + (sent,) * (groups - 1),
        in_specs=[VMEM, VMEM],
        out_specs=(VMEM,) * groups,
        compiler_params=pltpu.CompilerParams(vmem_limit_bytes=40 << 20),
        cost_estimate=pl.CostEstimate(flops=1 << 24, bytes_accessed=1 << 22, transcendentals=0),
        name="join_halves",
    )(mine, theirs)


def merge_kernel(lambdas, own, *refs):
    *parts, gain, out = refs
    for head in range(2):
        maps = []
        for which in range(2):
            kind = which * 2 + head
            levels, outcomes = [own[kind, WIDTH : WIDTH + 1, :]], [own[kind, :WIDTH, :]]
            for part in parts:
                stats = part[kind, WIDTH:, :].astype(F32)
                levels.append(stats[0:1] + stats[1:2] + stats[2:3])
                outcomes.append(part[kind, :WIDTH, :].astype(F32))
            top = functools.reduce(jnp.maximum, levels)
            weights = [jnp.exp2(level - top) for level in levels]
            total = sum(weights)
            maps.append(sum(o * (w / total) for o, w in zip(outcomes, weights)))
        attended = maps[0] - lambdas[head] * maps[1]
        mean_square = jnp.mean(attended * attended, axis=0, keepdims=True)
        normed = attended * lax.rsqrt(mean_square + 1e-05)
        out[:, head * WIDTH : (head + 1) * WIDTH] = (normed.T * gain[...]).astype(BF16)


def merge(lambdas, own, parts, gain):
    return pl.pallas_call(
        merge_kernel,
        out_shape=jax.ShapeDtypeStruct((COLS, 2 * WIDTH), BF16),
        in_specs=[SMEM] + [VMEM] * (2 + len(parts)),
        out_specs=VMEM,
        compiler_params=pltpu.CompilerParams(vmem_limit_bytes=8 << 20),
        cost_estimate=pl.CostEstimate(flops=1 << 22, bytes_accessed=1 << 21, transcendentals=0),
        name="merge",
    )(lambdas, own, *parts, gain.reshape(1, WIDTH))


def row_norm(rows, gain, epsilon):
    mean_square = jnp.mean(rows * rows, axis=-1, keepdims=True)
    return rows * lax.rsqrt(mean_square + epsilon) * gain


def project_kernel(me, h0, h1, h2, h3, r0, r1, r2, r3, weight, mixer_gain, before_gain, normed_out, stream_out, mixed, held, sems):
    group = h0.shape[1]
    quarter = r0.shape[0]
    copies = []
    for j in range(4):
        rows = pl.ds(pl.multiple_of(lax.rem(me[0] + j, 4) * group, group), group)
        copies.append(pltpu.make_async_copy(weight.at[rows, :], held.at[j], sems.at[j]))
        copies[j].start()
    for j, heads in enumerate((h0, h1, h2, h3)):
        copies[j].wait()
        term = jnp.dot(heads[...], held[j], preferred_element_type=F32)
        if j == 0:
            mixed[...] = term
        else:
            mixed[...] += term
    for k, residual in enumerate((r0, r1, r2, r3)):
        rows = pl.ds(pl.multiple_of(lax.rem(me[0] + k, 4) * quarter, quarter), quarter)
        block = mixed[rows, :].astype(BF16).astype(F32)
        stream = residual[...].astype(F32) + row_norm(block, mixer_gain[...], 1e-06)
        if k == 0:
            stream_out[...] = stream
        normed_out[k * quarter : (k + 1) * quarter, :] = row_norm(stream, before_gain[...], 1e-06).astype(BF16)


def project(me, heads, residuals, weight, mixer_gain, before_gain):
    tokens, width = heads[0].shape[0], weight.shape[1]
    return pl.pallas_call(
        project_kernel,
        out_shape=(
            jax.ShapeDtypeStruct((tokens, width), BF16),
            jax.ShapeDtypeStruct((tokens // 4, width), F32),
        ),
        in_specs=[SMEM] + [VMEM] * 8 + [HBM] + [VMEM] * 2,
        out_specs=(VMEM, VMEM),
        scratch_shapes=[
            pltpu.VMEM((tokens, width), F32),
            pltpu.VMEM((4, weight.shape[0] // 4, width), BF16),
            pltpu.SemaphoreType.DMA((4,)),
        ],
        compiler_params=pltpu.CompilerParams(vmem_limit_bytes=40 << 20),
        cost_estimate=pl.CostEstimate(
            flops=2 * tokens * width * weight.shape[0], bytes_accessed=8 << 20, transcendentals=0
        ),
        name="project",
    )(me, *heads, *residuals, weight, mixer_gain.reshape(1, width), before_gain.reshape(1, width))


CHUNK = 512
TALL_STEPS = 2


def mix_kernel(units, x, weights, o0, o1, o2, o3, held, hidden, gate_sems, down_sems):
    width = x.shape[1]
    tall = width // TALL_STEPS
    whole = units // CHUNK
    rest = units - whole * CHUNK

    def gate_up(i, start, cols):
        spans = [pl.ds(j * units + start, cols) for j in range(2)]
        return [
            pltpu.make_async_copy(weights.at[:, span], held.at[:, span], gate_sems.at[j, i])
            for j, span in enumerate(spans)
        ]

    def down(i, start):
        rows, cols = pl.ds(start, tall), pl.ds(2 * units, units)
        return pltpu.make_async_copy(weights.at[rows, cols], held.at[rows, cols], down_sems.at[i])

    for i in range(whole):
        for copy in gate_up(i, i * CHUNK, CHUNK):
            copy.start()
    if rest:
        for copy in gate_up(whole, whole * CHUNK, rest):
            copy.start()
    for i in range(TALL_STEPS):
        down(i, i * tall).start()

    def activate(i, start, cols):
        for copy in gate_up(i, start, cols):
            copy.wait()
        gate = jnp.dot(x[...], held[:, pl.ds(start, cols)], preferred_element_type=F32)
        up = jnp.dot(x[...], held[:, pl.ds(units + start, cols)], preferred_element_type=F32)
        hidden[:, pl.ds(start, cols)] = (gate / (1.0 + jnp.exp(-gate)) * up).astype(BF16)

    def gate_step(i, carry):
        activate(i, pl.multiple_of(i * CHUNK, CHUNK), CHUNK)
        return carry

    lax.fori_loop(0, whole, gate_step, 0)
    if rest:
        activate(whole, whole * CHUNK, rest)

    def down_step(i, carry):
        start = pl.multiple_of(i * tall, tall)
        down(i, start).wait()
        part = lax.dot_general(
            hidden[...],
            held[pl.ds(start, tall), 2 * units :],
            (((1,), (1,)), ((), ())),
            preferred_element_type=F32,
        ).astype(BF16)
        for k, out in enumerate((o0, o1, o2, o3)):
            rows = out.shape[0]
            out[:, pl.ds(start, tall)] = part[k * rows : (k + 1) * rows]
        return carry

    lax.fori_loop(0, TALL_STEPS, down_step, 0)


def mix(x, weights, units):
    tokens, width = x.shape
    shape = jax.ShapeDtypeStruct((tokens // 4, width), BF16)
    return pl.pallas_call(
        functools.partial(mix_kernel, units),
        out_shape=(shape,) * 4,
        in_specs=[VMEM, HBM],
        out_specs=(VMEM,) * 4,
        scratch_shapes=[
            pltpu.VMEM(weights.shape, BF16),
            pltpu.VMEM((tokens, units), BF16),
            pltpu.SemaphoreType.DMA((2, pl.cdiv(units, CHUNK))),
            pltpu.SemaphoreType.DMA((TALL_STEPS,)),
        ],
        compiler_params=pltpu.CompilerParams(vmem_limit_bytes=40 << 20),
        cost_estimate=pl.CostEstimate(
            flops=6 * tokens * width * units, bytes_accessed=6 * width * units, transcendentals=0
        ),
        name="mix",
    )(x, weights)


def pack_kernel(gate, up, down, out):
    units = gate.shape[1]
    out[:, :units] = gate[...]
    out[:, units : 2 * units] = up[...]
    out[:, 2 * units :] = down[...]


def pack(gate, up, down):
    return pl.pallas_call(
        pack_kernel,
        out_shape=jax.ShapeDtypeStruct((gate.shape[0], 3 * gate.shape[1]), BF16),
        in_specs=[VMEM] * 3,
        out_specs=VMEM,
        cost_estimate=pl.CostEstimate(flops=1 << 16, bytes_accessed=1 << 19, transcendentals=0),
        name="pack",
    )(gate, up, down.T)


def on_device(
    residual,
    queries,
    key_pairs,
    values,
    lambdas,
    head_gain,
    out_weight,
    mixer_gain,
    before_gain,
    after_gain,
    gate_weight,
    up_weight,
    down_weight,
):
    me = lax.axis_index(T).reshape(1)
    units = gate_weight.shape[1]
    packed = pack(gate_weight, up_weight, down_weight)
    packed, key_pairs, values, queries = lax.optimization_barrier((packed, key_pairs, values, queries))
    weights = lax.all_gather(packed, SP, axis=0, tiled=True)
    kv = jnp.concatenate((key_pairs, values), axis=1)
    beside = [(i, i ^ 1) for i in range(lax.axis_size(X))]
    kv = jnp.concatenate((kv, shifted(kv, X, 2)), axis=0)
    own_queries = jnp.concatenate((queries, lax.ppermute(queries, X, beside)), axis=0)
    queries = (own_queries, shifted(own_queries, C, 1))
    kv, queries = lax.optimization_barrier((kv, queries))
    carried, pieces = None, (kv,)
    above = below = kv
    for step in range(1, lax.axis_size(Z) // 2):
        above, below = shifted(above, Z, 1), shifted(below, Z, -1)
        carried = attend(carried, queries, pieces)
        carried, above, below, residual = lax.optimization_barrier((carried, above, below, residual))
        pieces = (above, below)
        if step == 2:
            residuals = [residual] + [shifted(residual, T, k) for k in (1, 2, 3)]
    half = kv.shape[0] // 2
    far = (shifted(above[:half], Z, 1), shifted(below[half:], Z, -1))
    carried = attend(carried, queries, pieces)
    carried, residuals = lax.optimization_barrier((carried, residuals))
    mine, theirs, _ = attend(carried, queries, far)
    own, sent = join_halves(mine, shifted(theirs, C, 1))
    head_out = merge(lambdas, own, [lax.ppermute(sent, X, beside)], head_gain)

    heads = [head_out] + [shifted(head_out, T, k) for k in (1, 2, 3)]
    normed_in, stream = project(me, heads, residuals, out_weight, mixer_gain, before_gain)
    parts = mix(normed_in, weights, units)
    arrived = [parts[0]] + [shifted(parts[k], T, -k) for k in (2, 1, 3)]
    channel = sum(part.astype(F32) for part in arrived).astype(BF16)
    updated = stream + 0.5 * row_norm(channel.astype(F32), after_gain, 1e-06)
    return updated.astype(BF16)


def solution(mesh):
    finer = Mesh(mesh.devices.reshape(8, 4, 2, mesh.shape[T]), SP_TP)
    in_specs = (
        P(SP_TP, None),
        P(SP, T),
        P(SP, T),
        P(SP, T),
        P(T),
        P(),
        P(),
        P(),
        P(),
        P(),
        P(SP, T),
        P(SP, T),
        P(T, SP),
    )
    return jax.shard_map(
        on_device, mesh=finer, in_specs=in_specs, out_specs=P(SP_TP, None), check_vma=False
    )
```

profile of v0, /device:TPU:228, one launch (start us, length us, event | category | flops | bytes accessed | tf_op | source)
XLA Modules:
  0.0 276.3 jit_solution(15238392225033318107)
XLA Ops:
  6.5 1.7 pack.1
  8.3 1.3 collective-permute-start.1
  11.4 2.5 collective-permute-done.1
  14.6 6.9 %collective-permute-done = bf16[256,256]{1,0:T(8,128)(2,1)S(1)} collective-permute-done((bf16[256,256]{1,0:T(8,128)(2,1)S(1)}, bf16[256,256]{1,0:T(8,128)(2,1)S(1)}, u32[]{:S(2)}, u32[]{:S(2)}) %collective-permute-start) | collective-permute-done | bytes 131104 | tf_op jit(solution)/shard_map/ppermute | solution.py:33
  21.5 1.1 collective-permute-start.3
  22.6 2.2 collective-permute-start.4
  24.8 5.8 %attend.5 = (f32[8,136,256]{2,1,0:T(8,128)S(1)}, f32[8,136,256]{2,1,0:T(8,128)S(1)}, bf16[16,256,256]{2,1,0:T(8,128)(2,1)S(1)}) custom-call(bf16[512,256]{1,0:T(8,128)(2,1)S(1)} %constant_dynamic-update-slice_fusion.2.refs_0_, bf16[512,256]{1,0:T(8,128)(2,1)S(1)} %collective-permute-done.2.refs_1_, bf16[512,256]{1,0:T(8,128)(2,1)S(1)} %pad_maximum_fusion.refs_2_), custom_call_target="tpu_custom_call" | custom-call | flops 2147483648 | bytes 2359296 | tf_op jit(solution)/shard_map/attend/pallas_call | solution.py:164
  30.6 2.4 collective-permute-done.3.refs_0_
  34.7 2.9 %collective-permute-start.6 = (bf16[512,256]{1,0:T(8,128)(2,1)S(1)}, bf16[512,256]{1,0:T(8,128)(2,1)S(1)}, u32[]{:S(2)}, u32[]{:S(2)}) collective-permute-start(bf16[512,256]{1,0:T(8,128)(2,1)S(1)} %collective-permute-done.4.refs_1_), channel_id=1, source_target_pairs={{224,0},{0,32},{32,64},{64,96},{96,128},{128,160},{160,192},{192,2... | collective-permute-start | bytes 786440 | tf_op jit(solution)/shard_map/ppermute | solution.py:33
  37.6 6.9 %attend.6 = (f32[8,136,256]{2,1,0:T(8,128)S(1)}, f32[8,136,256]{2,1,0:T(8,128)S(1)}) custom-call(bf16[512,256]{1,0:T(8,128)(2,1)S(1)} %collective-permute-done.3.refs_0_, bf16[512,256]{1,0:T(8,128)(2,1)S(1)} %collective-permute-done.4.refs_1_, f32[8,136,256]{2,1,0:T(8,128)S(1)} %get-tuple-element.66.refs_2_, f32[8,136,256]{2,1,0:T(8,128)S(1)} %get-tuple-element.67.refs_3_, ...), custom_call_target="tpu_custom_call" | custom-call | flops 4294967296 | bytes 2621440 | tf_op jit(solution)/shard_map/attend/pallas_call | solution.py:164
  44.5 2.3 collective-permute-done.5.refs_0_
  46.9 38.0 %collective-permute-start.11 = (bf16[64,2048]{1,0:T(8,128)(2,1)S(1)}, bf16[64,2048]{1,0:T(8,128)(2,1)S(1)}, u32[]{:S(2)}, u32[]{:S(2)}) collective-permute-start(bf16[64,2048]{1,0:T(8,128)(2,1)S(1)} %copy-done.1), channel_id=1, source_target_pairs={{1,0},{2,1},{3,2},{0,3},{5,4},{6,5},{7,6},{4,7},{9,8},{10,9},{11,1... | collective-permute-start | bytes 786440 | tf_op jit(solution)/shard_map/ppermute | solution.py:33
  85.8 13.7 %collective-permute-start.7 = (bf16[512,256]{1,0:T(8,128)(2,1)S(1)}, bf16[512,256]{1,0:T(8,128)(2,1)S(1)}, u32[]{:S(2)}, u32[]{:S(2)}) collective-permute-start(bf16[512,256]{1,0:T(8,128)(2,1)S(1)} %collective-permute-done.5.refs_0_), channel_id=1, source_target_pairs={{32,0},{64,32},{96,64},{128,96},{160,128},{192,160},{224,192},{0,2... | collective-permute-start | bytes 786440 | tf_op jit(solution)/shard_map/ppermute | solution.py:33
  99.5 6.9 %attend.7 = (f32[8,136,256]{2,1,0:T(8,128)S(1)}, f32[8,136,256]{2,1,0:T(8,128)S(1)}) custom-call(bf16[512,256]{1,0:T(8,128)(2,1)S(1)} %collective-permute-done.5.refs_0_, bf16[512,256]{1,0:T(8,128)(2,1)S(1)} %collective-permute-done.6.refs_1_, f32[8,136,256]{2,1,0:T(8,128)S(1)} %get-tuple-element.74.refs_2_, f32[8,136,256]{2,1,0:T(8,128)S(1)} %get-tuple-element.75.refs_3_, ...), custom_call_target="tpu_custom_call" | custom-call | flops 4294967296 | bytes 2621440 | tf_op jit(solution)/shard_map/attend/pallas_call | solution.py:164
  106.4 3.3 %collective-permute-done.7.refs_0_ = bf16[512,256]{1,0:T(8,128)(2,1)S(1)} collective-permute-done((bf16[512,256]{1,0:T(8,128)(2,1)S(1)}, bf16[512,256]{1,0:T(8,128)(2,1)S(1)}, u32[]{:S(2)}, u32[]{:S(2)}) %collective-permute-start.7) | collective-permute-done | bytes 262176 | tf_op jit(solution)/shard_map/ppermute | solution.py:33
  109.7 2.4 collective-permute-done.8.refs_1_
  112.1 34.0 %collective-permute-start.9 = (bf16[256,256]{1,0:T(8,128)(2,1)S(1)}, bf16[256,256]{1,0:T(8,128)(2,1)S(1)}, u32[]{:S(2)}, u32[]{:S(2)}) collective-permute-start(bf16[256,256]{1,0:T(8,128)(2,1)S(1)} %slice.6), channel_id=1, source_target_pairs={{32,0},{64,32},{96,64},{128,96},{160,128},{192,160},{224,192},{0,2... | collective-permute-start | bytes 393224 | tf_op jit(solution)/shard_map/ppermute | solution.py:33
  146.2 6.9 %attend.8 = (f32[8,136,256]{2,1,0:T(8,128)S(1)}, f32[8,136,256]{2,1,0:T(8,128)S(1)}) custom-call(bf16[512,256]{1,0:T(8,128)(2,1)S(1)} %collective-permute-done.7.refs_0_, bf16[512,256]{1,0:T(8,128)(2,1)S(1)} %collective-permute-done.8.refs_1_, f32[8,136,256]{2,1,0:T(8,128)S(1)} %get-tuple-element.82.refs_2_, f32[8,136,256]{2,1,0:T(8,128)S(1)} %get-tuple-element.83.refs_3_, ...), custom_call_target="tpu_custom_call" | custom-call | flops 4294967296 | bytes 2621440 | tf_op jit(solution)/shard_map/attend/pallas_call | solution.py:164
  153.2 4.7 %attend.9 = (f32[8,136,256]{2,1,0:T(8,128)S(1)}, f32[8,136,256]{2,1,0:T(8,128)S(1)}) custom-call(bf16[256,256]{1,0:T(8,128)(2,1)S(1)} %collective-permute-done.9.refs_0_, bf16[256,256]{1,0:T(8,128)(2,1)S(1)} %collective-permute-done.10.refs_1_, f32[8,136,256]{2,1,0:T(8,128)S(1)} %get-tuple-element.87.refs_2_, f32[8,136,256]{2,1,0:T(8,128)S(1)} %get-tuple-element.88.refs_3_, ...), custom_call_target="tpu_custom_call" | custom-call | flops 2147483648 | bytes 2359296 | tf_op jit(solution)/shard_map/attend/pallas_call | solution.py:164
  158.0 2.7 collective-permute-done.14.theirs
  161.1 9.0 %collective-permute-done.15.refs_0_ = bf16[4,144,256]{2,1,0:T(8,128)(2,1)S(1)} collective-permute-done((bf16[4,144,256]{2,1,0:T(8,128)(2,1)S(1)}, bf16[4,144,256]{2,1,0:T(8,128)(2,1)S(1)}, u32[]{:S(2)}, u32[]{:S(2)}) %collective-permute-start.15) | collective-permute-done | bytes 294944 | tf_op jit(solution)/shard_map/ppermute | solution.py:448
  170.9 61.1 %collective-permute-start.16 = (bf16[256,256]{1,0:T(8,128)(2,1)S(1)}, bf16[256,256]{1,0:T(8,128)(2,1)S(1)}, u32[]{:S(2)}, u32[]{:S(2)}) collective-permute-start(bf16[256,256]{1,0:T(8,128)(2,1)S(1)} %merge.1.h0), channel_id=1, source_target_pairs={{1,0},{2,1},{3,2},{0,3},{5,4},{6,5},{7,6},{4,7},{9,8},{10,9},{11,1... | collective-permute-start | bytes 393224 | tf_op jit(solution)/shard_map/ppermute | solution.py:33
  233.0 4.0 %collective-permute-done.16.h1 = bf16[256,256]{1,0:T(8,128)(2,1)S(1)} collective-permute-done((bf16[256,256]{1,0:T(8,128)(2,1)S(1)}, bf16[256,256]{1,0:T(8,128)(2,1)S(1)}, u32[]{:S(2)}, u32[]{:S(2)}) %collective-permute-start.16) | collective-permute-done | bytes 131104 | tf_op jit(solution)/shard_map/ppermute | solution.py:33
  237.0 2.3 collective-permute-done.17.h2
  239.4 1.1 collective-permute-done.18.h3
  240.5 2.2 copy-done
  242.6 2.7 project.1
  245.4 8.1 %mix.1 = (bf16[64,2048]{1,0:T(8,128)(2,1)S(1)}, bf16[64,2048]{1,0:T(8,128)(2,1)S(1)}, bf16[64,2048]{1,0:T(8,128)(2,1)S(1)}, bf16[64,2048]{1,0:T(8,128)(2,1)S(1)}) custom-call(bf16[256,2048]{1,0:T(8,128)(2,1)S(1)} %get-tuple-element.99.x, bf16[2048,4224]{1,0:T(8,128)(2,1)} %all-gather.2.cloned.1.call-done.weights), custom_call_target="tpu_custom_call" | custom-call | flops 4429185024 | bytes 17301504 | tf_op jit(solution)/shard_map/mix/pallas_call | solution.py:370
  253.5 1.0 collective-permute-start.21
  254.5 1.1 collective-permute-start.20
  256.3 6.5 %collective-permute-done.21 = bf16[64,2048]{1,0:T(8,128)(2,1)S(1)} collective-permute-done((bf16[64,2048]{1,0:T(8,128)(2,1)S(1)}, bf16[64,2048]{1,0:T(8,128)(2,1)S(1)}, u32[]{:S(2)}, u32[]{:S(2)}) %collective-permute-start.21) | collective-permute-done | bytes 262176 | tf_op jit(solution)/shard_map/ppermute | solution.py:33
  262.8 5.5 %collective-permute-done.20 = bf16[64,2048]{1,0:T(8,128)(2,1)S(1)} collective-permute-done((bf16[64,2048]{1,0:T(8,128)(2,1)S(1)}, bf16[64,2048]{1,0:T(8,128)(2,1)S(1)}, u32[]{:S(2)}, u32[]{:S(2)}) %collective-permute-start.20) | collective-permute-done | bytes 262176 | tf_op jit(solution)/shard_map/ppermute | solution.py:33
  (51 shorter events, 9.3 us)
Async XLA Ops:
  6.5 7.4 %copy-start.6 = (bf16[256,128]{1,0:T(8,128)(2,1)S(1)}, bf16[256,128]{1,0:T(8,128)(2,1)}, u32[]{:S(2)}) copy-start(bf16[256,128]{1,0:T(8,128)(2,1)} %param.16) | copy-start | bytes 196612
  6.5 238.8 %all-gather.2.cloned.1.call-start = ((), (), s32[]{:S(2)}) async-start(), calls=%async_computation | async-start | bytes 17571840 | tf_op jit(solution)/shard_map/all_gather | solution.py:426
  8.3 5.5 %collective-permute-start.1 = (bf16[256,256]{1,0:T(8,128)(2,1)}, bf16[256,256]{1,0:T(8,128)(2,1)S(1)}, u32[]{:S(2)}, u32[]{:S(2)}) collective-permute-start(bf16[256,256]{1,0:T(8,128)(2,1)} %param.14), channel_id=1, source_target_pairs={{0,8},{8,0},{16,24},{24,16},{1,9},{9,1},{17,25},{25,17},{2,10},{10... | collective-permute-start | bytes 393224 | tf_op jit(solution)/shard_map/ppermute | solution.py:430
  13.9 7.6 %collective-permute-start.2 = (bf16[512,256]{1,0:T(8,128)(2,1)S(1)}, bf16[512,256]{1,0:T(8,128)(2,1)S(1)}, u32[]{:S(2)}, u32[]{:S(2)}) collective-permute-start(bf16[512,256]{1,0:T(8,128)(2,1)S(1)} %constant_dynamic-update-slice_fusion.2.refs_0_), channel_id=1, source_target_pairs={{4,0},{0,4},{5,1},{1,5},{6,2},{2,6},{7,3},{3,7},{12,8},{8,12},{13,... | collective-permute-start | bytes 786440 | tf_op jit(solution)/shard_map/ppermute | solution.py:33
  14.0 7.5 %collective-permute-start = (bf16[256,256]{1,0:T(8,128)(2,1)S(1)}, bf16[256,256]{1,0:T(8,128)(2,1)S(1)}, u32[]{:S(2)}, u32[]{:S(2)}) collective-permute-start(bf16[256,256]{1,0:T(8,128)(2,1)S(1)} %constant_dynamic-update-slice_fusion), channel_id=1, source_target_pairs={{16,0},{24,8},{0,16},{8,24},{17,1},{25,9},{1,17},{9,25},{18,2},{26... | collective-permute-start | bytes 393224 | tf_op jit(solution)/shard_map/ppermute | solution.py:33
  21.5 11.5 %collective-permute-start.3 = (bf16[512,256]{1,0:T(8,128)(2,1)S(1)}, bf16[512,256]{1,0:T(8,128)(2,1)S(1)}, u32[]{:S(2)}, u32[]{:S(2)}) collective-permute-start(bf16[512,256]{1,0:T(8,128)(2,1)S(1)} %pad_maximum_fusion.refs_2_), channel_id=1, source_target_pairs={{32,0},{64,32},{96,64},{128,96},{160,128},{192,160},{224,192},{0,2... | collective-permute-start | bytes 786440 | tf_op jit(solution)/shard_map/ppermute | solution.py:33
  22.6 11.2 %collective-permute-start.4 = (bf16[512,256]{1,0:T(8,128)(2,1)S(1)}, bf16[512,256]{1,0:T(8,128)(2,1)S(1)}, u32[]{:S(2)}, u32[]{:S(2)}) collective-permute-start(bf16[512,256]{1,0:T(8,128)(2,1)S(1)} %pad_maximum_fusion.refs_2_), channel_id=1, source_target_pairs={{224,0},{0,32},{32,64},{64,96},{96,128},{128,160},{160,192},{192,2... | collective-permute-start | bytes 786440 | tf_op jit(solution)/shard_map/ppermute | solution.py:33
  33.8 13.0 %copy-start.1 = (bf16[64,2048]{1,0:T(8,128)(2,1)S(1)}, bf16[64,2048]{1,0:T(8,128)(2,1)}, u32[]{:S(2)}) copy-start(bf16[64,2048]{1,0:T(8,128)(2,1)} %r0) | copy-start | bytes 786436
  33.8 13.0 %collective-permute-start.5 = (bf16[512,256]{1,0:T(8,128)(2,1)S(1)}, bf16[512,256]{1,0:T(8,128)(2,1)S(1)}, u32[]{:S(2)}, u32[]{:S(2)}) collective-permute-start(bf16[512,256]{1,0:T(8,128)(2,1)S(1)} %collective-permute-done.3.refs_0_), channel_id=1, source_target_pairs={{32,0},{64,32},{96,64},{128,96},{160,128},{192,160},{224,192},{0,2... | collective-permute-start | bytes 786440 | tf_op jit(solution)/shard_map/ppermute | solution.py:33
  34.7 12.2 %collective-permute-start.6 = (bf16[512,256]{1,0:T(8,128)(2,1)S(1)}, bf16[512,256]{1,0:T(8,128)(2,1)S(1)}, u32[]{:S(2)}, u32[]{:S(2)}) collective-permute-start(bf16[512,256]{1,0:T(8,128)(2,1)S(1)} %collective-permute-done.4.refs_1_), channel_id=1, source_target_pairs={{224,0},{0,32},{32,64},{64,96},{96,128},{128,160},{160,192},{192,2... | collective-permute-start | bytes 786440 | tf_op jit(solution)/shard_map/ppermute | solution.py:33
  46.9 106.3 %collective-permute-start.11 = (bf16[64,2048]{1,0:T(8,128)(2,1)S(1)}, bf16[64,2048]{1,0:T(8,128)(2,1)S(1)}, u32[]{:S(2)}, u32[]{:S(2)}) collective-permute-start(bf16[64,2048]{1,0:T(8,128)(2,1)S(1)} %copy-done.1), channel_id=1, source_target_pairs={{1,0},{2,1},{3,2},{0,3},{5,4},{6,5},{7,6},{4,7},{9,8},{10,9},{11,1... | collective-permute-start | bytes 786440 | tf_op jit(solution)/shard_map/ppermute | solution.py:33
  84.9 68.3 %collective-permute-start.12 = (bf16[64,2048]{1,0:T(8,128)(2,1)S(1)}, bf16[64,2048]{1,0:T(8,128)(2,1)S(1)}, u32[]{:S(2)}, u32[]{:S(2)}) collective-permute-start(bf16[64,2048]{1,0:T(8,128)(2,1)S(1)} %copy-done.1), channel_id=1, source_target_pairs={{2,0},{3,1},{0,2},{1,3},{6,4},{7,5},{4,6},{5,7},{10,8},{11,9},{8,1... | collective-permute-start | bytes 786440 | tf_op jit(solution)/shard_map/ppermute | solution.py:33
  84.9 68.3 %collective-permute-start.13 = (bf16[64,2048]{1,0:T(8,128)(2,1)S(1)}, bf16[64,2048]{1,0:T(8,128)(2,1)S(1)}, u32[]{:S(2)}, u32[]{:S(2)}) collective-permute-start(bf16[64,2048]{1,0:T(8,128)(2,1)S(1)} %copy-done.1), channel_id=1, source_target_pairs={{3,0},{0,1},{1,2},{2,3},{7,4},{4,5},{5,6},{6,7},{11,8},{8,9},{9,10... | collective-permute-start | bytes 786440 | tf_op jit(solution)/shard_map/ppermute | solution.py:33
  85.8 23.9 %collective-permute-start.7 = (bf16[512,256]{1,0:T(8,128)(2,1)S(1)}, bf16[512,256]{1,0:T(8,128)(2,1)S(1)}, u32[]{:S(2)}, u32[]{:S(2)}) collective-permute-start(bf16[512,256]{1,0:T(8,128)(2,1)S(1)} %collective-permute-done.5.refs_0_), channel_id=1, source_target_pairs={{32,0},{64,32},{96,64},{128,96},{160,128},{192,160},{224,192},{0,2... | collective-permute-start | bytes 786440 | tf_op jit(solution)/shard_map/ppermute | solution.py:33
  99.5 12.6 %collective-permute-start.8 = (bf16[512,256]{1,0:T(8,128)(2,1)S(1)}, bf16[512,256]{1,0:T(8,128)(2,1)S(1)}, u32[]{:S(2)}, u32[]{:S(2)}) collective-permute-start(bf16[512,256]{1,0:T(8,128)(2,1)S(1)} %collective-permute-done.6.refs_1_), channel_id=1, source_target_pairs={{224,0},{0,32},{32,64},{64,96},{96,128},{128,160},{160,192},{192,2... | collective-permute-start | bytes 786440 | tf_op jit(solution)/shard_map/ppermute | solution.py:33
  112.1 41.0 %collective-permute-start.9 = (bf16[256,256]{1,0:T(8,128)(2,1)S(1)}, bf16[256,256]{1,0:T(8,128)(2,1)S(1)}, u32[]{:S(2)}, u32[]{:S(2)}) collective-permute-start(bf16[256,256]{1,0:T(8,128)(2,1)S(1)} %slice.6), channel_id=1, source_target_pairs={{32,0},{64,32},{96,64},{128,96},{160,128},{192,160},{224,192},{0,2... | collective-permute-start | bytes 393224 | tf_op jit(solution)/shard_map/ppermute | solution.py:33
  146.1 7.1 %collective-permute-start.10 = (bf16[256,256]{1,0:T(8,128)(2,1)S(1)}, bf16[256,256]{1,0:T(8,128)(2,1)S(1)}, u32[]{:S(2)}, u32[]{:S(2)}) collective-permute-start(bf16[256,256]{1,0:T(8,128)(2,1)S(1)} %slice.7), channel_id=1, source_target_pairs={{224,0},{0,32},{32,64},{64,96},{96,128},{128,160},{160,192},{192,2... | collective-permute-start | bytes 393224 | tf_op jit(solution)/shard_map/ppermute | solution.py:33
  157.9 2.8 %collective-permute-start.14 = (f32[8,136,256]{2,1,0:T(8,128)S(1)}, f32[8,136,256]{2,1,0:T(8,128)S(1)}, u32[]{:S(2)}, u32[]{:S(2)}) collective-permute-start(f32[8,136,256]{2,1,0:T(8,128)S(1)} %get-tuple-element.91), channel_id=1, source_target_pairs={{4,0},{0,4},{5,1},{1,5},{6,2},{2,6},{7,3},{3,7},{12,8},{8,12},{13,... | collective-permute-start | bytes 3342344 | tf_op jit(solution)/shard_map/ppermute | solution.py:33
  160.7 9.4 %copy-start.4 = (f32[2]{0:T(128)S(1)}, f32[2]{0:T(128)}, u32[]{:S(2)}) copy-start(f32[2]{0:T(128)} %lambdas.1) | copy-start | bytes 28
  160.7 9.4 %copy-start.5 = (f32[128]{0:T(128)S(1)}, f32[128]{0:T(128)}, u32[]{:S(2)}) copy-start(f32[128]{0:T(128)} %param.18) | copy-start | bytes 1540
  160.7 79.7 %copy-start.2 = (f32[2048]{0:T(1024)S(1)}, f32[2048]{0:T(1024)}, u32[]{:S(2)}) copy-start(f32[2048]{0:T(1024)} %param.20) | copy-start | bytes 24580
  160.8 79.7 %copy-start.3 = (f32[2048]{0:T(1024)S(1)}, f32[2048]{0:T(1024)}, u32[]{:S(2)}) copy-start(f32[2048]{0:T(1024)} %param.21) | copy-start | bytes 24580
  161.0 9.1 %collective-permute-start.15 = (bf16[4,144,256]{2,1,0:T(8,128)(2,1)S(1)}, bf16[4,144,256]{2,1,0:T(8,128)(2,1)S(1)}, u32[]{:S(2)}, u32[]{:S(2)}) collective-permute-start(bf16[4,144,256]{2,1,0:T(8,128)(2,1)S(1)} %get-tuple-element.93), channel_id=1, source_target_pairs={{0,8},{8,0},{16,24},{24,16},{1,9},{9,1},{17,25},{25,17},{2,10},{10... | collective-permute-start | bytes 884744 | tf_op jit(solution)/shard_map/ppermute | solution.py:448
  170.9 66.1 %collective-permute-start.16 = (bf16[256,256]{1,0:T(8,128)(2,1)S(1)}, bf16[256,256]{1,0:T(8,128)(2,1)S(1)}, u32[]{:S(2)}, u32[]{:S(2)}) collective-permute-start(bf16[256,256]{1,0:T(8,128)(2,1)S(1)} %merge.1.h0), channel_id=1, source_target_pairs={{1,0},{2,1},{3,2},{0,3},{5,4},{6,5},{7,6},{4,7},{9,8},{10,9},{11,1... | collective-permute-start | bytes 393224 | tf_op jit(solution)/shard_map/ppermute | solution.py:33
  232.0 7.4 %collective-permute-start.17 = (bf16[256,256]{1,0:T(8,128)(2,1)S(1)}, bf16[256,256]{1,0:T(8,128)(2,1)S(1)}, u32[]{:S(2)}, u32[]{:S(2)}) collective-permute-start(bf16[256,256]{1,0:T(8,128)(2,1)S(1)} %merge.1.h0), channel_id=1, source_target_pairs={{2,0},{3,1},{0,2},{1,3},{6,4},{7,5},{4,6},{5,7},{10,8},{11,9},{8,1... | collective-permute-start | bytes 393224 | tf_op jit(solution)/shard_map/ppermute | solution.py:33
  232.0 8.4 %collective-permute-start.18 = (bf16[256,256]{1,0:T(8,128)(2,1)S(1)}, bf16[256,256]{1,0:T(8,128)(2,1)S(1)}, u32[]{:S(2)}, u32[]{:S(2)}) collective-permute-start(bf16[256,256]{1,0:T(8,128)(2,1)S(1)} %merge.1.h0), channel_id=1, source_target_pairs={{3,0},{0,1},{1,2},{2,3},{7,4},{4,5},{5,6},{6,7},{11,8},{8,9},{9,10... | collective-permute-start | bytes 393224 | tf_op jit(solution)/shard_map/ppermute | solution.py:33
  240.5 2.2 copy-start
  253.5 15.1 %copy-start.7 = (f32[2048]{0:T(1024)S(1)}, f32[2048]{0:T(1024)}, u32[]{:S(2)}) copy-start(f32[2048]{0:T(1024)} %param.22) | copy-start | bytes 24580
  253.5 9.3 %collective-permute-start.21 = (bf16[64,2048]{1,0:T(8,128)(2,1)S(1)}, bf16[64,2048]{1,0:T(8,128)(2,1)S(1)}, u32[]{:S(2)}, u32[]{:S(2)}) collective-permute-start(bf16[64,2048]{1,0:T(8,128)(2,1)S(1)} %get-tuple-element.104), channel_id=1, source_target_pairs={{1,0},{2,1},{3,2},{0,3},{5,4},{6,5},{7,6},{4,7},{9,8},{10,9},{11,1... | collective-permute-start | bytes 786440 | tf_op jit(solution)/shard_map/ppermute | solution.py:33
  254.5 13.8 %collective-permute-start.20 = (bf16[64,2048]{1,0:T(8,128)(2,1)S(1)}, bf16[64,2048]{1,0:T(8,128)(2,1)S(1)}, u32[]{:S(2)}, u32[]{:S(2)}) collective-permute-start(bf16[64,2048]{1,0:T(8,128)(2,1)S(1)} %get-tuple-element.103), channel_id=1, source_target_pairs={{3,0},{0,1},{1,2},{2,3},{7,4},{4,5},{5,6},{6,7},{11,8},{8,9},{9,10... | collective-permute-start | bytes 786440 | tf_op jit(solution)/shard_map/ppermute | solution.py:33
  255.6 12.7 %collective-permute-start.19 = (bf16[64,2048]{1,0:T(8,128)(2,1)S(1)}, bf16[64,2048]{1,0:T(8,128)(2,1)S(1)}, u32[]{:S(2)}, u32[]{:S(2)}) collective-permute-start(bf16[64,2048]{1,0:T(8,128)(2,1)S(1)} %get-tuple-element.102), channel_id=1, source_target_pairs={{2,0},{3,1},{0,2},{1,3},{6,4},{7,5},{4,6},{5,7},{10,8},{11,9},{8,1... | collective-permute-start | bytes 786440 | tf_op jit(solution)/shard_map/ppermute | solution.py:33
Sparse Core Ops, SparseCore 0:
  10.1 105.5 all-gather.1
where the time goes:
time: 278 us; the launch traced here: 276 us
  starting transfers between devices  161 us (58%)
  waiting for transfers between devices  51.9 us (19%)
  Pallas kernels  44.9 us (16%)
  between operations  13.6 us (5%)
  local copies, waits for them, and re-layouts  4.03 us (1%)
    ppermute x20, starting transfers between devices, shifted(): lax.ppermute(array, axis, [((i + by) % count, i) for i in range(count)])  159 us
    ppermute x20, waiting for transfers between devices, shifted(): lax.ppermute(array, axis, [((i + by) % count, i) for i in range(count)])  40.4 us
    pallas_call x5, Pallas kernels, attend(): pl.pallas_call(functools.partial(attend_kernel, first, len(kvs), groups),...  31.3 us
    ppermute x1, waiting for transfers between devices, on_device(): head_out = merge(lambdas, own, [lax.ppermute(sent, X, beside)], head_gain)  9.03 us
    pallas_call x1, Pallas kernels, mix(): pl.pallas_call(functools.partial(mix_kernel, units), out_shape=(shape,) *...  8.13 us
  transfers between devices with their start and end apart: 23, of which 14 were waited for; matrix products, arithmetic and copies ran while one was open for 1% of the time, Pallas kernels for 13%

commit v1 on v0

--- a/solution.py
+++ b/solution.py
@@ -178,76 +178,78 @@
     return done if first else (*done, carried[2])
 
 
-def halves_kernel(mine, theirs, own, *sent):
-    line = lax.broadcasted_iota(jnp.int32, (8, COLS), 0)
-
-    def joined(tile):
-        a, b = mine.at[tile], theirs.at[tile]
-        top_a, top_b = a[WIDTH : WIDTH + 1, :], b[WIDTH : WIDTH + 1, :]
-        top = jnp.maximum(top_a, top_b)
-        weight_a, weight_b = jnp.exp2(top_a - top), jnp.exp2(top_b - top)
-        total = a[WIDTH + 1 : WIDTH + 2, :] * weight_a + b[WIDTH + 1 : WIDTH + 2, :] * weight_b
-        return (a[:WIDTH, :] * weight_a + b[:WIDTH, :] * weight_b) / total, top + jnp.log2(total)
-
-    for kind in range(4):
-        outcome, level = joined(kind)
-        own[kind, :WIDTH, :] = outcome
-        own[kind, WIDTH:, :] = jnp.broadcast_to(level, (8, COLS))
-        for group, out in enumerate(sent):
-            outcome, level = joined(4 * (group + 1) + kind)
-            out[kind, :WIDTH, :] = outcome.astype(BF16)
-            high = level.astype(BF16).astype(F32)
-            middle = (level - high).astype(BF16).astype(F32)
-            low = level - high - middle
-            parts = jnp.where(line == 0, high, jnp.where(line == 1, middle, low))
-            out[kind, WIDTH:, :] = jnp.concatenate((parts, jnp.zeros_like(parts)), axis=0).astype(BF16)
-
-
-def join_halves(mine, theirs):
-    groups = mine.shape[0] // 4
-    sent = jax.ShapeDtypeStruct((4, TALL, COLS), BF16)
-    return pl.pallas_call(
-        halves_kernel,
-        out_shape=(jax.ShapeDtypeStruct((4, STATE, COLS), F32),) + (sent,) * (groups - 1),
+def joined(mine, theirs, tile):
+    a, b = mine[tile, WIDTH:, :], theirs[tile, WIDTH:, :]
+    top = jnp.maximum(a[0:1], b[0:1])
+    weight_a, weight_b = jnp.exp2(a[0:1] - top), jnp.exp2(b[0:1] - top)
+    total = a[1:2] * weight_a + b[1:2] * weight_b
+    return weight_a, weight_b, total, top + jnp.log2(total)
+
+
+def levels_kernel(mine, theirs, out):
+    for tile in range(8):
+        out[tile : tile + 1, :] = joined(mine, theirs, tile)[3]
+
+
+def levels_of(mine, theirs):
+    return pl.pallas_call(
+        levels_kernel,
+        out_shape=jax.ShapeDtypeStruct((8, COLS), F32),
         in_specs=[VMEM, VMEM],
-        out_specs=(VMEM,) * groups,
-        compiler_params=pltpu.CompilerParams(vmem_limit_bytes=40 << 20),
-        cost_estimate=pl.CostEstimate(flops=1 << 24, bytes_accessed=1 << 22, transcendentals=0),
-        name="join_halves",
+        out_specs=VMEM,
+        compiler_params=pltpu.CompilerParams(vmem_limit_bytes=8 << 20),
+        cost_estimate=pl.CostEstimate(flops=1 << 18, bytes_accessed=1 << 16, transcendentals=0),
+        name="levels",
     )(mine, theirs)
 
 
-def merge_kernel(lambdas, own, *refs):
-    *parts, gain, out = refs
+def differ_kernel(lambdas, mine, theirs, levels, levels_beside, own, sent):
+    for group, out in enumerate((own, sent)):
+        for head in range(2):
+            shares = []
+            for which in range(2):
+                kind = which * 2 + head
+                tile, same = 4 * group + kind, 4 * (1 - group) + kind
+                here, there = levels[tile : tile + 1, :], levels_beside[same : same + 1, :]
+                top = jnp.maximum(here, there)
+                share = jnp.exp2(here - top) / (jnp.exp2(here - top) + jnp.exp2(there - top))
+                weight_a, weight_b, total, _ = joined(mine, theirs, tile)
+                share = share / total
+                shares.append(mine[tile, :WIDTH, :] * (weight_a * share) + theirs[tile, :WIDTH, :] * (weight_b * share))
+            out[head] = (shares[0] - lambdas[head] * shares[1]).astype(out.dtype)
+
+
+def differ(lambdas, mine, theirs, levels, levels_beside):
+    shape = (2, WIDTH, COLS)
+    return pl.pallas_call(
+        differ_kernel,
+        out_shape=(jax.ShapeDtypeStruct(shape, F32), jax.ShapeDtypeStruct(shape, BF16)),
+        in_specs=[SMEM] + [VMEM] * 4,
+        out_specs=(VMEM, VMEM),
+        compiler_params=pltpu.CompilerParams(vmem_limit_bytes=8 << 20),
+        cost_estimate=pl.CostEstimate(flops=1 << 22, bytes_accessed=1 << 21, transcendentals=0),
+        name="differ",
+    )(lambdas, mine, theirs, levels, levels_beside)
+
+
+def merge_kernel(own, arrived, gain, out):
     for head in range(2):
-        maps = []
-        for which in range(2):
-            kind = which * 2 + head
-            levels, outcomes = [own[kind, WIDTH : WIDTH + 1, :]], [own[kind, :WIDTH, :]]
-            for part in parts:
-                stats = part[kind, WIDTH:, :].astype(F32)
-                levels.append(stats[0:1] + stats[1:2] + stats[2:3])
-                outcomes.append(part[kind, :WIDTH, :].astype(F32))
-            top = functools.reduce(jnp.maximum, levels)
-            weights = [jnp.exp2(level - top) for level in levels]
-            total = sum(weights)
-            maps.append(sum(o * (w / total) for o, w in zip(outcomes, weights)))
-        attended = maps[0] - lambdas[head] * maps[1]
+        attended = own[head] + arrived[head].astype(F32)
         mean_square = jnp.mean(attended * attended, axis=0, keepdims=True)
         normed = attended * lax.rsqrt(mean_square + 1e-05)
         out[:, head * WIDTH : (head + 1) * WIDTH] = (normed.T * gain[...]).astype(BF16)
 
 
-def merge(lambdas, own, parts, gain):
+def merge(own, arrived, gain):
     return pl.pallas_call(
         merge_kernel,
         out_shape=jax.ShapeDtypeStruct((COLS, 2 * WIDTH), BF16),
-        in_specs=[SMEM] + [VMEM] * (2 + len(parts)),
+        in_specs=[VMEM] * 3,
         out_specs=VMEM,
         compiler_params=pltpu.CompilerParams(vmem_limit_bytes=8 << 20),
         cost_estimate=pl.CostEstimate(flops=1 << 22, bytes_accessed=1 << 21, transcendentals=0),
         name="merge",
-    )(lambdas, own, *parts, gain.reshape(1, WIDTH))
+    )(own, arrived, gain.reshape(1, WIDTH))
 
 
 def row_norm(rows, gain, epsilon):
@@ -444,8 +446,10 @@
     carried = attend(carried, queries, pieces)
     carried, residuals = lax.optimization_barrier((carried, residuals))
     mine, theirs, _ = attend(carried, queries, far)
-    own, sent = join_halves(mine, shifted(theirs, C, 1))
-    head_out = merge(lambdas, own, [lax.ppermute(sent, X, beside)], head_gain)
+    theirs = shifted(theirs, C, 1)
+    levels = levels_of(mine, theirs)
+    own, sent = differ(lambdas, mine, theirs, levels, lax.ppermute(levels, X, beside))
+    head_out = merge(own, lax.ppermute(sent, X, beside), head_gain)
 
     heads = [head_out] + [shifted(head_out, T, k) for k in (1, 2, 3)]
     normed_in, stream = project(me, heads, residuals, out_weight, mixer_gain, before_gain)

time: 278 us -> 278 us (level)
  the two profiles are of different devices: /device:TPU:228 before, /device:TPU:4 now
where the time goes in v1:
time: 278 us; the launch traced here: 279 us
  starting transfers between devices  154 us (55%)
  Pallas kernels  63.9 us (23%)
  waiting for transfers between devices  42 us (15%)
  between operations  13.6 us (5%)
  local copies, waits for them, and re-layouts  4.04 us (1%)
    ppermute x20, starting transfers between devices, shifted(): lax.ppermute(array, axis, [((i + by) % count, i) for i in range(count)])  93.8 us
    ppermute x1, starting transfers between devices, on_device(): lax.ppermute(levels, X, beside)  56.8 us
    pallas_call x5, Pallas kernels, attend(): pl.pallas_call(functools.partial(attend_kernel, first, len(kvs), groups),...  50.4 us
    ppermute x20, waiting for transfers between devices, shifted(): lax.ppermute(array, axis, [((i + by) % count, i) for i in range(count)])  35 us
    pallas_call x1, Pallas kernels, mix(): pl.pallas_call(functools.partial(mix_kernel, units), out_shape=(shape,) *...  8.13 us
  transfers between devices with their start and end apart: 24, of which 15 were waited for; matrix products, arithmetic and copies ran while one was open for 1% of the time, Pallas kernels for 19%

profile of v1, /device:TPU:4, one launch (start us, length us, event | category | flops | bytes accessed | tf_op | source)
XLA Modules:
  0.0 278.8 jit_solution(12332851964887818525)
XLA Ops:
  6.5 1.7 pack.1
  8.3 1.3 collective-permute-start.1
  11.4 2.5 collective-permute-done.1
  14.0 2.0 collective-permute-start
  16.0 5.4 %collective-permute-done = bf16[256,256]{1,0:T(8,128)(2,1)S(1)} collective-permute-done((bf16[256,256]{1,0:T(8,128)(2,1)S(1)}, bf16[256,256]{1,0:T(8,128)(2,1)S(1)}, u32[]{:S(2)}, u32[]{:S(2)}) %collective-permute-start) | collective-permute-done | bytes 131104 | tf_op jit(solution)/shard_map/ppermute | solution.py:33
  21.5 5.9 %collective-permute-start.3 = (bf16[512,256]{1,0:T(8,128)(2,1)S(1)}, bf16[512,256]{1,0:T(8,128)(2,1)S(1)}, u32[]{:S(2)}, u32[]{:S(2)}) collective-permute-start(bf16[512,256]{1,0:T(8,128)(2,1)S(1)} %pad_maximum_fusion.refs_2_), channel_id=1, source_target_pairs={{32,0},{64,32},{96,64},{128,96},{160,128},{192,160},{224,192},{0,2... | collective-permute-start | bytes 786440 | tf_op jit(solution)/shard_map/ppermute | solution.py:33
  27.4 5.8 %attend.5 = (f32[8,136,256]{2,1,0:T(8,128)S(1)}, f32[8,136,256]{2,1,0:T(8,128)S(1)}, bf16[16,256,256]{2,1,0:T(8,128)(2,1)S(1)}) custom-call(bf16[512,256]{1,0:T(8,128)(2,1)S(1)} %constant_dynamic-update-slice_fusion.2.refs_0_, bf16[512,256]{1,0:T(8,128)(2,1)S(1)} %collective-permute-done.2.refs_1_, bf16[512,256]{1,0:T(8,128)(2,1)S(1)} %pad_maximum_fusion.refs_2_), custom_call_target="tpu_custom_call" | custom-call | flops 2147483648 | bytes 2359296 | tf_op jit(solution)/shard_map/attend/pallas_call | solution.py:164
  33.2 1.9 collective-permute-done.3.refs_0_
  35.2 5.0 %collective-permute-done.4.refs_1_ = bf16[512,256]{1,0:T(8,128)(2,1)S(1)} collective-permute-done((bf16[512,256]{1,0:T(8,128)(2,1)S(1)}, bf16[512,256]{1,0:T(8,128)(2,1)S(1)}, u32[]{:S(2)}, u32[]{:S(2)}) %collective-permute-start.4) | collective-permute-done | bytes 262176 | tf_op jit(solution)/shard_map/ppermute | solution.py:33
  40.2 2.0 collective-permute-start.6
  42.2 6.9 %attend.6 = (f32[8,136,256]{2,1,0:T(8,128)S(1)}, f32[8,136,256]{2,1,0:T(8,128)S(1)}) custom-call(bf16[512,256]{1,0:T(8,128)(2,1)S(1)} %collective-permute-done.3.refs_0_, bf16[512,256]{1,0:T(8,128)(2,1)S(1)} %collective-permute-done.4.refs_1_, f32[8,136,256]{2,1,0:T(8,128)S(1)} %get-tuple-element.66.refs_2_, f32[8,136,256]{2,1,0:T(8,128)S(1)} %get-tuple-element.67.refs_3_, ...), custom_call_target="tpu_custom_call" | custom-call | flops 4294967296 | bytes 2621440 | tf_op jit(solution)/shard_map/attend/pallas_call | solution.py:164
  49.2 2.4 collective-permute-done.5.refs_0_
  52.3 37.2 %collective-permute-start.11 = (bf16[64,2048]{1,0:T(8,128)(2,1)S(1)}, bf16[64,2048]{1,0:T(8,128)(2,1)S(1)}, u32[]{:S(2)}, u32[]{:S(2)}) collective-permute-start(bf16[64,2048]{1,0:T(8,128)(2,1)S(1)} %copy-done.1), channel_id=1, source_target_pairs={{1,0},{2,1},{3,2},{0,3},{5,4},{6,5},{7,6},{4,7},{9,8},{10,9},{11,1... | collective-permute-start | bytes 786440 | tf_op jit(solution)/shard_map/ppermute | solution.py:33
  90.5 16.3 %collective-permute-start.7 = (bf16[512,256]{1,0:T(8,128)(2,1)S(1)}, bf16[512,256]{1,0:T(8,128)(2,1)S(1)}, u32[]{:S(2)}, u32[]{:S(2)}) collective-permute-start(bf16[512,256]{1,0:T(8,128)(2,1)S(1)} %collective-permute-done.5.refs_0_), channel_id=1, source_target_pairs={{32,0},{64,32},{96,64},{128,96},{160,128},{192,160},{224,192},{0,2... | collective-permute-start | bytes 786440 | tf_op jit(solution)/shard_map/ppermute | solution.py:33
  106.8 6.9 %attend.7 = (f32[8,136,256]{2,1,0:T(8,128)S(1)}, f32[8,136,256]{2,1,0:T(8,128)S(1)}) custom-call(bf16[512,256]{1,0:T(8,128)(2,1)S(1)} %collective-permute-done.5.refs_0_, bf16[512,256]{1,0:T(8,128)(2,1)S(1)} %collective-permute-done.6.refs_1_, f32[8,136,256]{2,1,0:T(8,128)S(1)} %get-tuple-element.74.refs_2_, f32[8,136,256]{2,1,0:T(8,128)S(1)} %get-tuple-element.75.refs_3_, ...), custom_call_target="tpu_custom_call" | custom-call | flops 4294967296 | bytes 2621440 | tf_op jit(solution)/shard_map/attend/pallas_call | solution.py:164
  114.3 2.7 collective-permute-start.9
  117.1 6.9 %attend.8 = (f32[8,136,256]{2,1,0:T(8,128)S(1)}, f32[8,136,256]{2,1,0:T(8,128)S(1)}) custom-call(bf16[512,256]{1,0:T(8,128)(2,1)S(1)} %collective-permute-done.7.refs_0_, bf16[512,256]{1,0:T(8,128)(2,1)S(1)} %collective-permute-done.8.refs_1_, f32[8,136,256]{2,1,0:T(8,128)S(1)} %get-tuple-element.82.refs_2_, f32[8,136,256]{2,1,0:T(8,128)S(1)} %get-tuple-element.83.refs_3_, ...), custom_call_target="tpu_custom_call" | custom-call | flops 4294967296 | bytes 2621440 | tf_op jit(solution)/shard_map/attend/pallas_call | solution.py:164
  124.1 23.8 %attend.9 = (f32[8,136,256]{2,1,0:T(8,128)S(1)}, f32[8,136,256]{2,1,0:T(8,128)S(1)}) custom-call(bf16[256,256]{1,0:T(8,128)(2,1)S(1)} %collective-permute-done.9.refs_0_, bf16[256,256]{1,0:T(8,128)(2,1)S(1)} %collective-permute-done.10.refs_1_, f32[8,136,256]{2,1,0:T(8,128)S(1)} %get-tuple-element.87.refs_2_, f32[8,136,256]{2,1,0:T(8,128)S(1)} %get-tuple-element.88.refs_3_, ...), custom_call_target="tpu_custom_call" | custom-call | flops 2147483648 | bytes 2359296 | tf_op jit(solution)/shard_map/attend/pallas_call | solution.py:164
  148.0 2.7 collective-permute-done.14.theirs
  150.8 56.8 %collective-permute-start.15 = (f32[8,256]{1,0:T(8,128)S(1)}, f32[8,256]{1,0:T(8,128)S(1)}, u32[]{:S(2)}, u32[]{:S(2)}) collective-permute-start(f32[8,256]{1,0:T(8,128)S(1)} %levels.1), channel_id=1, source_target_pairs={{0,8},{8,0},{16,24},{24,16},{1,9},{9,1},{17,25},{25,17},{2,10},{10... | collective-permute-start | bytes 24584 | tf_op jit(solution)/shard_map/ppermute | solution.py:451
  207.7 1.6 collective-permute-done.15.levels_beside
  210.1 2.1 collective-permute-start.16
  212.2 2.9 %collective-permute-done.16.arrived = bf16[2,128,256]{2,1,0:T(8,128)(2,1)S(1)} collective-permute-done((bf16[2,128,256]{2,1,0:T(8,128)(2,1)S(1)}, bf16[2,128,256]{2,1,0:T(8,128)(2,1)S(1)}, u32[]{:S(2)}, u32[]{:S(2)}) %collective-permute-start.16) | collective-permute-done | bytes 131104 | tf_op jit(solution)/shard_map/ppermute | solution.py:452
  215.3 22.4 %collective-permute-start.17 = (bf16[256,256]{1,0:T(8,128)(2,1)S(1)}, bf16[256,256]{1,0:T(8,128)(2,1)S(1)}, u32[]{:S(2)}, u32[]{:S(2)}) collective-permute-start(bf16[256,256]{1,0:T(8,128)(2,1)S(1)} %merge.1.h0), channel_id=1, source_target_pairs={{1,0},{2,1},{3,2},{0,3},{5,4},{6,5},{7,6},{4,7},{9,8},{10,9},{11,1... | collective-permute-start | bytes 393224 | tf_op jit(solution)/shard_map/ppermute | solution.py:33
  238.7 3.0 %collective-permute-done.17.h1 = bf16[256,256]{1,0:T(8,128)(2,1)S(1)} collective-permute-done((bf16[256,256]{1,0:T(8,128)(2,1)S(1)}, bf16[256,256]{1,0:T(8,128)(2,1)S(1)}, u32[]{:S(2)}, u32[]{:S(2)}) %collective-permute-start.17) | collective-permute-done | bytes 131104 | tf_op jit(solution)/shard_map/ppermute | solution.py:33
  241.6 2.6 collective-permute-done.18.h2
  245.3 2.2 copy-done
  247.5 2.7 project.1
  250.2 8.1 %mix.1 = (bf16[64,2048]{1,0:T(8,128)(2,1)S(1)}, bf16[64,2048]{1,0:T(8,128)(2,1)S(1)}, bf16[64,2048]{1,0:T(8,128)(2,1)S(1)}, bf16[64,2048]{1,0:T(8,128)(2,1)S(1)}) custom-call(bf16[256,2048]{1,0:T(8,128)(2,1)S(1)} %get-tuple-element.99.x, bf16[2048,4224]{1,0:T(8,128)(2,1)} %all-gather.2.cloned.1.call-done.weights), custom_call_target="tpu_custom_call" | custom-call | flops 4429185024 | bytes 17301504 | tf_op jit(solution)/shard_map/mix/pallas_call | solution.py:372
  259.3 1.1 collective-permute-start.21
  261.4 4.5 %collective-permute-done.22 = bf16[64,2048]{1,0:T(8,128)(2,1)S(1)} collective-permute-done((bf16[64,2048]{1,0:T(8,128)(2,1)S(1)}, bf16[64,2048]{1,0:T(8,128)(2,1)S(1)}, u32[]{:S(2)}, u32[]{:S(2)}) %collective-permute-start.22) | collective-permute-done | bytes 262176 | tf_op jit(solution)/shard_map/ppermute | solution.py:33
  265.9 4.9 %collective-permute-done.21 = bf16[64,2048]{1,0:T(8,128)(2,1)S(1)} collective-permute-done((bf16[64,2048]{1,0:T(8,128)(2,1)S(1)}, bf16[64,2048]{1,0:T(8,128)(2,1)S(1)}, u32[]{:S(2)}, u32[]{:S(2)}) %collective-permute-start.21) | collective-permute-done | bytes 262176 | tf_op jit(solution)/shard_map/ppermute | solution.py:33
  (54 shorter events, 10.4 us)
Async XLA Ops:
  6.5 7.4 %copy-start.6 = (bf16[256,128]{1,0:T(8,128)(2,1)S(1)}, bf16[256,128]{1,0:T(8,128)(2,1)}, u32[]{:S(2)}) copy-start(bf16[256,128]{1,0:T(8,128)(2,1)} %param.16) | copy-start | bytes 196612
  6.5 243.7 %all-gather.2.cloned.1.call-start = ((), (), s32[]{:S(2)}) async-start(), calls=%async_computation | async-start | bytes 17571840 | tf_op jit(solution)/shard_map/all_gather | solution.py:428
  8.3 5.5 %collective-permute-start.1 = (bf16[256,256]{1,0:T(8,128)(2,1)}, bf16[256,256]{1,0:T(8,128)(2,1)S(1)}, u32[]{:S(2)}, u32[]{:S(2)}) collective-permute-start(bf16[256,256]{1,0:T(8,128)(2,1)} %param.14), channel_id=1, source_target_pairs={{0,8},{8,0},{16,24},{24,16},{1,9},{9,1},{17,25},{25,17},{2,10},{10... | collective-permute-start | bytes 393224 | tf_op jit(solution)/shard_map/ppermute | solution.py:432
  13.8 7.6 %collective-permute-start.2 = (bf16[512,256]{1,0:T(8,128)(2,1)S(1)}, bf16[512,256]{1,0:T(8,128)(2,1)S(1)}, u32[]{:S(2)}, u32[]{:S(2)}) collective-permute-start(bf16[512,256]{1,0:T(8,128)(2,1)S(1)} %constant_dynamic-update-slice_fusion.2.refs_0_), channel_id=1, source_target_pairs={{4,0},{0,4},{5,1},{1,5},{6,2},{2,6},{7,3},{3,7},{12,8},{8,12},{13,... | collective-permute-start | bytes 786440 | tf_op jit(solution)/shard_map/ppermute | solution.py:33
  14.0 7.5 %collective-permute-start = (bf16[256,256]{1,0:T(8,128)(2,1)S(1)}, bf16[256,256]{1,0:T(8,128)(2,1)S(1)}, u32[]{:S(2)}, u32[]{:S(2)}) collective-permute-start(bf16[256,256]{1,0:T(8,128)(2,1)S(1)} %constant_dynamic-update-slice_fusion), channel_id=1, source_target_pairs={{16,0},{24,8},{0,16},{8,24},{17,1},{25,9},{1,17},{9,25},{18,2},{26... | collective-permute-start | bytes 393224 | tf_op jit(solution)/shard_map/ppermute | solution.py:33
  21.5 13.7 %collective-permute-start.3 = (bf16[512,256]{1,0:T(8,128)(2,1)S(1)}, bf16[512,256]{1,0:T(8,128)(2,1)S(1)}, u32[]{:S(2)}, u32[]{:S(2)}) collective-permute-start(bf16[512,256]{1,0:T(8,128)(2,1)S(1)} %pad_maximum_fusion.refs_2_), channel_id=1, source_target_pairs={{32,0},{64,32},{96,64},{128,96},{160,128},{192,160},{224,192},{0,2... | collective-permute-start | bytes 786440 | tf_op jit(solution)/shard_map/ppermute | solution.py:33
  27.4 12.8 %collective-permute-start.4 = (bf16[512,256]{1,0:T(8,128)(2,1)S(1)}, bf16[512,256]{1,0:T(8,128)(2,1)S(1)}, u32[]{:S(2)}, u32[]{:S(2)}) collective-permute-start(bf16[512,256]{1,0:T(8,128)(2,1)S(1)} %pad_maximum_fusion.refs_2_), channel_id=1, source_target_pairs={{224,0},{0,32},{32,64},{64,96},{96,128},{128,160},{160,192},{192,2... | collective-permute-start | bytes 786440 | tf_op jit(solution)/shard_map/ppermute | solution.py:33
  40.2 12.1 %copy-start.1 = (bf16[64,2048]{1,0:T(8,128)(2,1)S(1)}, bf16[64,2048]{1,0:T(8,128)(2,1)}, u32[]{:S(2)}) copy-start(bf16[64,2048]{1,0:T(8,128)(2,1)} %r0) | copy-start | bytes 786436
  40.2 11.4 %collective-permute-start.5 = (bf16[512,256]{1,0:T(8,128)(2,1)S(1)}, bf16[512,256]{1,0:T(8,128)(2,1)S(1)}, u32[]{:S(2)}, u32[]{:S(2)}) collective-permute-start(bf16[512,256]{1,0:T(8,128)(2,1)S(1)} %collective-permute-done.3.refs_0_), channel_id=1, source_target_pairs={{32,0},{64,32},{96,64},{128,96},{160,128},{192,160},{224,192},{0,2... | collective-permute-start | bytes 786440 | tf_op jit(solution)/shard_map/ppermute | solution.py:33
  40.2 12.1 %collective-permute-start.6 = (bf16[512,256]{1,0:T(8,128)(2,1)S(1)}, bf16[512,256]{1,0:T(8,128)(2,1)S(1)}, u32[]{:S(2)}, u32[]{:S(2)}) collective-permute-start(bf16[512,256]{1,0:T(8,128)(2,1)S(1)} %collective-permute-done.4.refs_1_), channel_id=1, source_target_pairs={{224,0},{0,32},{32,64},{64,96},{96,128},{128,160},{160,192},{192,2... | collective-permute-start | bytes 786440 | tf_op jit(solution)/shard_map/ppermute | solution.py:33
  52.3 71.8 %collective-permute-start.11 = (bf16[64,2048]{1,0:T(8,128)(2,1)S(1)}, bf16[64,2048]{1,0:T(8,128)(2,1)S(1)}, u32[]{:S(2)}, u32[]{:S(2)}) collective-permute-start(bf16[64,2048]{1,0:T(8,128)(2,1)S(1)} %copy-done.1), channel_id=1, source_target_pairs={{1,0},{2,1},{3,2},{0,3},{5,4},{6,5},{7,6},{4,7},{9,8},{10,9},{11,1... | collective-permute-start | bytes 786440 | tf_op jit(solution)/shard_map/ppermute | solution.py:33
  89.5 34.6 %collective-permute-start.12 = (bf16[64,2048]{1,0:T(8,128)(2,1)S(1)}, bf16[64,2048]{1,0:T(8,128)(2,1)S(1)}, u32[]{:S(2)}, u32[]{:S(2)}) collective-permute-start(bf16[64,2048]{1,0:T(8,128)(2,1)S(1)} %copy-done.1), channel_id=1, source_target_pairs={{2,0},{3,1},{0,2},{1,3},{6,4},{7,5},{4,6},{5,7},{10,8},{11,9},{8,1... | collective-permute-start | bytes 786440 | tf_op jit(solution)/shard_map/ppermute | solution.py:33
  89.5 34.6 %collective-permute-start.13 = (bf16[64,2048]{1,0:T(8,128)(2,1)S(1)}, bf16[64,2048]{1,0:T(8,128)(2,1)S(1)}, u32[]{:S(2)}, u32[]{:S(2)}) collective-permute-start(bf16[64,2048]{1,0:T(8,128)(2,1)S(1)} %copy-done.1), channel_id=1, source_target_pairs={{3,0},{0,1},{1,2},{2,3},{7,4},{4,5},{5,6},{6,7},{11,8},{8,9},{9,10... | collective-permute-start | bytes 786440 | tf_op jit(solution)/shard_map/ppermute | solution.py:33
  90.5 23.2 %collective-permute-start.7 = (bf16[512,256]{1,0:T(8,128)(2,1)S(1)}, bf16[512,256]{1,0:T(8,128)(2,1)S(1)}, u32[]{:S(2)}, u32[]{:S(2)}) collective-permute-start(bf16[512,256]{1,0:T(8,128)(2,1)S(1)} %collective-permute-done.5.refs_0_), channel_id=1, source_target_pairs={{32,0},{64,32},{96,64},{128,96},{160,128},{192,160},{224,192},{0,2... | collective-permute-start | bytes 786440 | tf_op jit(solution)/shard_map/ppermute | solution.py:33
  106.7 7.6 %collective-permute-start.8 = (bf16[512,256]{1,0:T(8,128)(2,1)S(1)}, bf16[512,256]{1,0:T(8,128)(2,1)S(1)}, u32[]{:S(2)}, u32[]{:S(2)}) collective-permute-start(bf16[512,256]{1,0:T(8,128)(2,1)S(1)} %collective-permute-done.6.refs_1_), channel_id=1, source_target_pairs={{224,0},{0,32},{32,64},{64,96},{96,128},{128,160},{160,192},{192,2... | collective-permute-start | bytes 786440 | tf_op jit(solution)/shard_map/ppermute | solution.py:33
  114.3 9.8 %collective-permute-start.9 = (bf16[256,256]{1,0:T(8,128)(2,1)S(1)}, bf16[256,256]{1,0:T(8,128)(2,1)S(1)}, u32[]{:S(2)}, u32[]{:S(2)}) collective-permute-start(bf16[256,256]{1,0:T(8,128)(2,1)S(1)} %slice.6), channel_id=1, source_target_pairs={{32,0},{64,32},{96,64},{128,96},{160,128},{192,160},{224,192},{0,2... | collective-permute-start | bytes 393224 | tf_op jit(solution)/shard_map/ppermute | solution.py:33
  117.1 7.1 %collective-permute-start.10 = (bf16[256,256]{1,0:T(8,128)(2,1)S(1)}, bf16[256,256]{1,0:T(8,128)(2,1)S(1)}, u32[]{:S(2)}, u32[]{:S(2)}) collective-permute-start(bf16[256,256]{1,0:T(8,128)(2,1)S(1)} %slice.7), channel_id=1, source_target_pairs={{224,0},{0,32},{32,64},{64,96},{96,128},{128,160},{160,192},{192,2... | collective-permute-start | bytes 393224 | tf_op jit(solution)/shard_map/ppermute | solution.py:33
  147.9 2.8 %collective-permute-start.14 = (f32[8,136,256]{2,1,0:T(8,128)S(1)}, f32[8,136,256]{2,1,0:T(8,128)S(1)}, u32[]{:S(2)}, u32[]{:S(2)}) collective-permute-start(f32[8,136,256]{2,1,0:T(8,128)S(1)} %get-tuple-element.91), channel_id=1, source_target_pairs={{4,0},{0,4},{5,1},{1,5},{6,2},{2,6},{7,3},{3,7},{12,8},{8,12},{13,... | collective-permute-start | bytes 3342344 | tf_op jit(solution)/shard_map/ppermute | solution.py:33
  150.7 58.6 %copy-start.4 = (f32[2]{0:T(128)S(1)}, f32[2]{0:T(128)}, u32[]{:S(2)}) copy-start(f32[2]{0:T(128)} %lambdas.1) | copy-start | bytes 28
  150.8 64.3 %copy-start.5 = (f32[128]{0:T(128)S(1)}, f32[128]{0:T(128)}, u32[]{:S(2)}) copy-start(f32[128]{0:T(128)} %param.18) | copy-start | bytes 1540
  150.8 94.5 %copy-start.2 = (f32[2048]{0:T(1024)S(1)}, f32[2048]{0:T(1024)}, u32[]{:S(2)}) copy-start(f32[2048]{0:T(1024)} %param.20) | copy-start | bytes 24580
  150.8 94.5 %copy-start.3 = (f32[2048]{0:T(1024)S(1)}, f32[2048]{0:T(1024)}, u32[]{:S(2)}) copy-start(f32[2048]{0:T(1024)} %param.21) | copy-start | bytes 24580
  150.8 58.5 %collective-permute-start.15 = (f32[8,256]{1,0:T(8,128)S(1)}, f32[8,256]{1,0:T(8,128)S(1)}, u32[]{:S(2)}, u32[]{:S(2)}) collective-permute-start(f32[8,256]{1,0:T(8,128)S(1)} %levels.1), channel_id=1, source_target_pairs={{0,8},{8,0},{16,24},{24,16},{1,9},{9,1},{17,25},{25,17},{2,10},{10... | collective-permute-start | bytes 24584 | tf_op jit(solution)/shard_map/ppermute | solution.py:451
  210.1 5.1 %collective-permute-start.16 = (bf16[2,128,256]{2,1,0:T(8,128)(2,1)S(1)}, bf16[2,128,256]{2,1,0:T(8,128)(2,1)S(1)}, u32[]{:S(2)}, u32[]{:S(2)}) collective-permute-start(bf16[2,128,256]{2,1,0:T(8,128)(2,1)S(1)} %get-tuple-element.93), channel_id=1, source_target_pairs={{0,8},{8,0},{16,24},{24,16},{1,9},{9,1},{17,25},{25,17},{2,10},{10... | collective-permute-start | bytes 393224 | tf_op jit(solution)/shard_map/ppermute | solution.py:452
  215.3 26.3 %collective-permute-start.17 = (bf16[256,256]{1,0:T(8,128)(2,1)S(1)}, bf16[256,256]{1,0:T(8,128)(2,1)S(1)}, u32[]{:S(2)}, u32[]{:S(2)}) collective-permute-start(bf16[256,256]{1,0:T(8,128)(2,1)S(1)} %merge.1.h0), channel_id=1, source_target_pairs={{1,0},{2,1},{3,2},{0,3},{5,4},{6,5},{7,6},{4,7},{9,8},{10,9},{11,1... | collective-permute-start | bytes 393224 | tf_op jit(solution)/shard_map/ppermute | solution.py:33
  237.7 6.6 %collective-permute-start.18 = (bf16[256,256]{1,0:T(8,128)(2,1)S(1)}, bf16[256,256]{1,0:T(8,128)(2,1)S(1)}, u32[]{:S(2)}, u32[]{:S(2)}) collective-permute-start(bf16[256,256]{1,0:T(8,128)(2,1)S(1)} %merge.1.h0), channel_id=1, source_target_pairs={{2,0},{3,1},{0,2},{1,3},{6,4},{7,5},{4,6},{5,7},{10,8},{11,9},{8,1... | collective-permute-start | bytes 393224 | tf_op jit(solution)/shard_map/ppermute | solution.py:33
  237.7 7.6 %collective-permute-start.19 = (bf16[256,256]{1,0:T(8,128)(2,1)S(1)}, bf16[256,256]{1,0:T(8,128)(2,1)S(1)}, u32[]{:S(2)}, u32[]{:S(2)}) collective-permute-start(bf16[256,256]{1,0:T(8,128)(2,1)S(1)} %merge.1.h0), channel_id=1, source_target_pairs={{3,0},{0,1},{1,2},{2,3},{7,4},{4,5},{5,6},{6,7},{11,8},{8,9},{9,10... | collective-permute-start | bytes 393224 | tf_op jit(solution)/shard_map/ppermute | solution.py:33
  245.3 2.2 copy-start
  258.4 12.7 %copy-start.7 = (f32[2048]{0:T(1024)S(1)}, f32[2048]{0:T(1024)}, u32[]{:S(2)}) copy-start(f32[2048]{0:T(1024)} %param.22) | copy-start | bytes 24580
  258.4 7.5 %collective-permute-start.22 = (bf16[64,2048]{1,0:T(8,128)(2,1)S(1)}, bf16[64,2048]{1,0:T(8,128)(2,1)S(1)}, u32[]{:S(2)}, u32[]{:S(2)}) collective-permute-start(bf16[64,2048]{1,0:T(8,128)(2,1)S(1)} %get-tuple-element.104), channel_id=1, source_target_pairs={{1,0},{2,1},{3,2},{0,3},{5,4},{6,5},{7,6},{4,7},{9,8},{10,9},{11,1... | collective-permute-start | bytes 786440 | tf_op jit(solution)/shard_map/ppermute | solution.py:33
  259.3 11.5 %collective-permute-start.21 = (bf16[64,2048]{1,0:T(8,128)(2,1)S(1)}, bf16[64,2048]{1,0:T(8,128)(2,1)S(1)}, u32[]{:S(2)}, u32[]{:S(2)}) collective-permute-start(bf16[64,2048]{1,0:T(8,128)(2,1)S(1)} %get-tuple-element.103), channel_id=1, source_target_pairs={{3,0},{0,1},{1,2},{2,3},{7,4},{4,5},{5,6},{6,7},{11,8},{8,9},{9,10... | collective-permute-start | bytes 786440 | tf_op jit(solution)/shard_map/ppermute | solution.py:33
  260.5 10.3 %collective-permute-start.20 = (bf16[64,2048]{1,0:T(8,128)(2,1)S(1)}, bf16[64,2048]{1,0:T(8,128)(2,1)S(1)}, u32[]{:S(2)}, u32[]{:S(2)}) collective-permute-start(bf16[64,2048]{1,0:T(8,128)(2,1)S(1)} %get-tuple-element.102), channel_id=1, source_target_pairs={{2,0},{3,1},{0,2},{1,3},{6,4},{7,5},{4,6},{5,7},{10,8},{11,9},{8,1... | collective-permute-start | bytes 786440 | tf_op jit(solution)/shard_map/ppermute | solution.py:33
Sparse Core Ops, SparseCore 0:
  10.1 104.7 all-gather.1

commit v2 on v1

--- a/solution.py
+++ b/solution.py
@@ -454,7 +454,7 @@
     heads = [head_out] + [shifted(head_out, T, k) for k in (1, 2, 3)]
     normed_in, stream = project(me, heads, residuals, out_weight, mixer_gain, before_gain)
     parts = mix(normed_in, weights, units)
-    arrived = [parts[0]] + [shifted(parts[k], T, -k) for k in (2, 1, 3)]
+    arrived = [parts[0]] + [shifted(parts[k], T, -k) for k in (1, 3, 2)]
     channel = sum(part.astype(F32) for part in arrived).astype(BF16)
     updated = stream + 0.5 * row_norm(channel.astype(F32), after_gain, 1e-06)
     return updated.astype(BF16)

time: 278 us -> 275 us (0.989)
  Pallas kernels: 63.9 us -> 195 us
  starting transfers between devices: 154 us -> 26.2 us
  waiting for transfers between devices: 42 us -> 35.3 us
    pallas_call x5, Pallas kernels: 50.4 us -> 182 us  [attend(): pl.pallas_call(functools.partial(attend_kernel, first, len(kvs), groups),...]
    ppermute x20, starting transfers between devices: 93.8 us -> 24.7 us  [shifted(): lax.ppermute(array, axis, [((i + by) % count, i) for i in range(count)])]
    ppermute x1, starting transfers between devices: 56.8 us -> 0.09 us  [on_device(): lax.ppermute(levels, X, beside)]
    ppermute x20, waiting for transfers between devices: 35 us -> 24.2 us  [shifted(): lax.ppermute(array, axis, [((i + by) % count, i) for i in range(count)])]
  transfers between devices with their start and end apart: 24 -> 24, of which waited for: 15 -> 11; matrix products, arithmetic and copies ran while one was open for 1% -> 1% of each run, Pallas kernels for 19% -> 67%
where the time goes in v2:
time: 275 us; the launch traced here: 276 us
  Pallas kernels  195 us (71%)
  waiting for transfers between devices  35.3 us (13%)
  starting transfers between devices  26.2 us (10%)
  between operations  13.7 us (5%)
  local copies, waits for them, and re-layouts  4.04 us (1%)
    pallas_call x5, Pallas kernels, attend(): pl.pallas_call(functools.partial(attend_kernel, first, len(kvs), groups),...  182 us
    ppermute x20, starting transfers between devices, shifted(): lax.ppermute(array, axis, [((i + by) % count, i) for i in range(count)])  24.7 us
    ppermute x20, waiting for transfers between devices, shifted(): lax.ppermute(array, axis, [((i + by) % count, i) for i in range(count)])  24.2 us
    pallas_call x1, Pallas kernels, mix(): pl.pallas_call(functools.partial(mix_kernel, units), out_shape=(shape,) *...  8.13 us
  transfers between devices with their start and end apart: 24, of which 11 were waited for; matrix products, arithmetic and copies ran while one was open for 1% of the time, Pallas kernels for 67%

profile of v2, /device:TPU:4, one launch (start us, length us, event | category | flops | bytes accessed | tf_op | source)
XLA Modules:
  0.0 275.6 jit_solution(9741479404877181480)
XLA Ops:
  6.5 1.7 pack.1
  8.3 1.3 collective-permute-start.1
  10.4 0.9 constant_dynamic-update-slice_fusion.3
  11.4 2.5 collective-permute-done.1
  14.0 2.0 collective-permute-start
  16.0 5.4 %collective-permute-done = bf16[256,256]{1,0:T(8,128)(2,1)S(1)} collective-permute-done((bf16[256,256]{1,0:T(8,128)(2,1)S(1)}, bf16[256,256]{1,0:T(8,128)(2,1)S(1)}, u32[]{:S(2)}, u32[]{:S(2)}) %collective-permute-start) | collective-permute-done | bytes 131104 | tf_op jit(solution)/shard_map/ppermute | solution.py:33
  21.5 5.9 %collective-permute-start.3 = (bf16[512,256]{1,0:T(8,128)(2,1)S(1)}, bf16[512,256]{1,0:T(8,128)(2,1)S(1)}, u32[]{:S(2)}, u32[]{:S(2)}) collective-permute-start(bf16[512,256]{1,0:T(8,128)(2,1)S(1)} %pad_maximum_fusion.refs_2_), channel_id=1, source_target_pairs={{32,0},{64,32},{96,64},{128,96},{160,128},{192,160},{224,192},{0,2... | collective-permute-start | bytes 786440 | tf_op jit(solution)/shard_map/ppermute | solution.py:33
  27.4 24.5 %attend.5 = (f32[8,136,256]{2,1,0:T(8,128)S(1)}, f32[8,136,256]{2,1,0:T(8,128)S(1)}, bf16[16,256,256]{2,1,0:T(8,128)(2,1)S(1)}) custom-call(bf16[512,256]{1,0:T(8,128)(2,1)S(1)} %constant_dynamic-update-slice_fusion.2.refs_0_, bf16[512,256]{1,0:T(8,128)(2,1)S(1)} %collective-permute-done.2.refs_1_, bf16[512,256]{1,0:T(8,128)(2,1)S(1)} %pad_maximum_fusion.refs_2_), custom_call_target="tpu_custom_call" | custom-call | flops 2147483648 | bytes 2359296 | tf_op jit(solution)/shard_map/attend/pallas_call | solution.py:164
  52.1 2.0 collective-permute-start.6
  54.1 44.5 %attend.6 = (f32[8,136,256]{2,1,0:T(8,128)S(1)}, f32[8,136,256]{2,1,0:T(8,128)S(1)}) custom-call(bf16[512,256]{1,0:T(8,128)(2,1)S(1)} %collective-permute-done.3.refs_0_, bf16[512,256]{1,0:T(8,128)(2,1)S(1)} %collective-permute-done.4.refs_1_, f32[8,136,256]{2,1,0:T(8,128)S(1)} %get-tuple-element.66.refs_2_, f32[8,136,256]{2,1,0:T(8,128)S(1)} %get-tuple-element.67.refs_3_, ...), custom_call_target="tpu_custom_call" | custom-call | flops 4294967296 | bytes 2621440 | tf_op jit(solution)/shard_map/attend/pallas_call | solution.py:164
  98.8 1.9 collective-permute-start.13
  100.7 2.0 collective-permute-start.8
  102.7 44.4 %attend.7 = (f32[8,136,256]{2,1,0:T(8,128)S(1)}, f32[8,136,256]{2,1,0:T(8,128)S(1)}) custom-call(bf16[512,256]{1,0:T(8,128)(2,1)S(1)} %collective-permute-done.5.refs_0_, bf16[512,256]{1,0:T(8,128)(2,1)S(1)} %collective-permute-done.6.refs_1_, f32[8,136,256]{2,1,0:T(8,128)S(1)} %get-tuple-element.74.refs_2_, f32[8,136,256]{2,1,0:T(8,128)S(1)} %get-tuple-element.75.refs_3_, ...), custom_call_target="tpu_custom_call" | custom-call | flops 4294967296 | bytes 2621440 | tf_op jit(solution)/shard_map/attend/pallas_call | solution.py:164
  147.3 2.1 collective-permute-start.10
  149.4 44.5 %attend.8 = (f32[8,136,256]{2,1,0:T(8,128)S(1)}, f32[8,136,256]{2,1,0:T(8,128)S(1)}) custom-call(bf16[512,256]{1,0:T(8,128)(2,1)S(1)} %collective-permute-done.7.refs_0_, bf16[512,256]{1,0:T(8,128)(2,1)S(1)} %collective-permute-done.8.refs_1_, f32[8,136,256]{2,1,0:T(8,128)S(1)} %get-tuple-element.82.refs_2_, f32[8,136,256]{2,1,0:T(8,128)S(1)} %get-tuple-element.83.refs_3_, ...), custom_call_target="tpu_custom_call" | custom-call | flops 4294967296 | bytes 2621440 | tf_op jit(solution)/shard_map/attend/pallas_call | solution.py:164
  193.9 23.8 %attend.9 = (f32[8,136,256]{2,1,0:T(8,128)S(1)}, f32[8,136,256]{2,1,0:T(8,128)S(1)}) custom-call(bf16[256,256]{1,0:T(8,128)(2,1)S(1)} %collective-permute-done.9.refs_0_, bf16[256,256]{1,0:T(8,128)(2,1)S(1)} %collective-permute-done.10.refs_1_, f32[8,136,256]{2,1,0:T(8,128)S(1)} %get-tuple-element.87.refs_2_, f32[8,136,256]{2,1,0:T(8,128)S(1)} %get-tuple-element.88.refs_3_, ...), custom_call_target="tpu_custom_call" | custom-call | flops 2147483648 | bytes 2359296 | tf_op jit(solution)/shard_map/attend/pallas_call | solution.py:164
  217.8 2.7 collective-permute-done.14.theirs
  220.7 3.6 %collective-permute-done.15.levels_beside = f32[8,256]{1,0:T(8,128)S(1)} collective-permute-done((f32[8,256]{1,0:T(8,128)S(1)}, f32[8,256]{1,0:T(8,128)S(1)}, u32[]{:S(2)}, u32[]{:S(2)}) %collective-permute-start.15) | collective-permute-done | bytes 8224 | tf_op jit(solution)/shard_map/ppermute | solution.py:451
  225.2 5.0 %collective-permute-done.16.arrived = bf16[2,128,256]{2,1,0:T(8,128)(2,1)S(1)} collective-permute-done((bf16[2,128,256]{2,1,0:T(8,128)(2,1)S(1)}, bf16[2,128,256]{2,1,0:T(8,128)(2,1)S(1)}, u32[]{:S(2)}, u32[]{:S(2)}) %collective-permute-start.16) | collective-permute-done | bytes 131104 | tf_op jit(solution)/shard_map/ppermute | solution.py:452
  230.4 4.2 %collective-permute-start.17 = (bf16[256,256]{1,0:T(8,128)(2,1)S(1)}, bf16[256,256]{1,0:T(8,128)(2,1)S(1)}, u32[]{:S(2)}, u32[]{:S(2)}) collective-permute-start(bf16[256,256]{1,0:T(8,128)(2,1)S(1)} %merge.1.h0), channel_id=1, source_target_pairs={{1,0},{2,1},{3,2},{0,3},{5,4},{6,5},{7,6},{4,7},{9,8},{10,9},{11,1... | collective-permute-start | bytes 393224 | tf_op jit(solution)/shard_map/ppermute | solution.py:33
  234.6 1.0 collective-permute-start.19
  235.5 3.2 %collective-permute-done.17.h1 = bf16[256,256]{1,0:T(8,128)(2,1)S(1)} collective-permute-done((bf16[256,256]{1,0:T(8,128)(2,1)S(1)}, bf16[256,256]{1,0:T(8,128)(2,1)S(1)}, u32[]{:S(2)}, u32[]{:S(2)}) %collective-permute-start.17) | collective-permute-done | bytes 131104 | tf_op jit(solution)/shard_map/ppermute | solution.py:33
  238.7 2.5 collective-permute-done.18.h2
  241.1 1.0 collective-permute-done.19.h3
  242.1 2.2 copy-done
  244.3 2.7 project.1
  247.1 8.1 %mix.1 = (bf16[64,2048]{1,0:T(8,128)(2,1)S(1)}, bf16[64,2048]{1,0:T(8,128)(2,1)S(1)}, bf16[64,2048]{1,0:T(8,128)(2,1)S(1)}, bf16[64,2048]{1,0:T(8,128)(2,1)S(1)}) custom-call(bf16[256,2048]{1,0:T(8,128)(2,1)S(1)} %get-tuple-element.99.x, bf16[2048,4224]{1,0:T(8,128)(2,1)} %all-gather.2.cloned.1.call-done.weights), custom_call_target="tpu_custom_call" | custom-call | flops 4429185024 | bytes 17301504 | tf_op jit(solution)/shard_map/mix/pallas_call | solution.py:372
  255.2 1.0 collective-permute-start.22
  257.0 1.3 collective-permute-start.20
  258.2 6.6 %collective-permute-done.22 = bf16[64,2048]{1,0:T(8,128)(2,1)S(1)} collective-permute-done((bf16[64,2048]{1,0:T(8,128)(2,1)S(1)}, bf16[64,2048]{1,0:T(8,128)(2,1)S(1)}, u32[]{:S(2)}, u32[]{:S(2)}) %collective-permute-start.22) | collective-permute-done | bytes 262176 | tf_op jit(solution)/shard_map/ppermute | solution.py:33
  264.9 1.2 collective-permute-done.21
  266.1 1.4 collective-permute-done.20
  (54 shorter events, 4.6 us)
Async XLA Ops:
  6.5 7.4 %copy-start.6 = (bf16[256,128]{1,0:T(8,128)(2,1)S(1)}, bf16[256,128]{1,0:T(8,128)(2,1)}, u32[]{:S(2)}) copy-start(bf16[256,128]{1,0:T(8,128)(2,1)} %param.16) | copy-start | bytes 196612
  6.5 240.5 %all-gather.2.cloned.1.call-start = ((), (), s32[]{:S(2)}) async-start(), calls=%async_computation | async-start | bytes 17571840 | tf_op jit(solution)/shard_map/all_gather | solution.py:428
  8.3 5.5 %collective-permute-start.1 = (bf16[256,256]{1,0:T(8,128)(2,1)}, bf16[256,256]{1,0:T(8,128)(2,1)S(1)}, u32[]{:S(2)}, u32[]{:S(2)}) collective-permute-start(bf16[256,256]{1,0:T(8,128)(2,1)} %param.14), channel_id=1, source_target_pairs={{0,8},{8,0},{16,24},{24,16},{1,9},{9,1},{17,25},{25,17},{2,10},{10... | collective-permute-start | bytes 393224 | tf_op jit(solution)/shard_map/ppermute | solution.py:432
  13.8 7.6 %collective-permute-start.2 = (bf16[512,256]{1,0:T(8,128)(2,1)S(1)}, bf16[512,256]{1,0:T(8,128)(2,1)S(1)}, u32[]{:S(2)}, u32[]{:S(2)}) collective-permute-start(bf16[512,256]{1,0:T(8,128)(2,1)S(1)} %constant_dynamic-update-slice_fusion.2.refs_0_), channel_id=1, source_target_pairs={{4,0},{0,4},{5,1},{1,5},{6,2},{2,6},{7,3},{3,7},{12,8},{8,12},{13,... | collective-permute-start | bytes 786440 | tf_op jit(solution)/shard_map/ppermute | solution.py:33
  14.0 7.5 %collective-permute-start = (bf16[256,256]{1,0:T(8,128)(2,1)S(1)}, bf16[256,256]{1,0:T(8,128)(2,1)S(1)}, u32[]{:S(2)}, u32[]{:S(2)}) collective-permute-start(bf16[256,256]{1,0:T(8,128)(2,1)S(1)} %constant_dynamic-update-slice_fusion), channel_id=1, source_target_pairs={{16,0},{24,8},{0,16},{8,24},{17,1},{25,9},{1,17},{9,25},{18,2},{26... | collective-permute-start | bytes 393224 | tf_op jit(solution)/shard_map/ppermute | solution.py:33
  21.5 30.5 %collective-permute-start.3 = (bf16[512,256]{1,0:T(8,128)(2,1)S(1)}, bf16[512,256]{1,0:T(8,128)(2,1)S(1)}, u32[]{:S(2)}, u32[]{:S(2)}) collective-permute-start(bf16[512,256]{1,0:T(8,128)(2,1)S(1)} %pad_maximum_fusion.refs_2_), channel_id=1, source_target_pairs={{32,0},{64,32},{96,64},{128,96},{160,128},{192,160},{224,192},{0,2... | collective-permute-start | bytes 786440 | tf_op jit(solution)/shard_map/ppermute | solution.py:33
  27.4 24.5 %collective-permute-start.4 = (bf16[512,256]{1,0:T(8,128)(2,1)S(1)}, bf16[512,256]{1,0:T(8,128)(2,1)S(1)}, u32[]{:S(2)}, u32[]{:S(2)}) collective-permute-start(bf16[512,256]{1,0:T(8,128)(2,1)S(1)} %pad_maximum_fusion.refs_2_), channel_id=1, source_target_pairs={{224,0},{0,32},{32,64},{64,96},{96,128},{128,160},{160,192},{192,2... | collective-permute-start | bytes 786440 | tf_op jit(solution)/shard_map/ppermute | solution.py:33
  52.0 46.6 %copy-start.1 = (bf16[64,2048]{1,0:T(8,128)(2,1)S(1)}, bf16[64,2048]{1,0:T(8,128)(2,1)}, u32[]{:S(2)}) copy-start(bf16[64,2048]{1,0:T(8,128)(2,1)} %r0) | copy-start | bytes 786436
  52.0 46.6 %collective-permute-start.5 = (bf16[512,256]{1,0:T(8,128)(2,1)S(1)}, bf16[512,256]{1,0:T(8,128)(2,1)S(1)}, u32[]{:S(2)}, u32[]{:S(2)}) collective-permute-start(bf16[512,256]{1,0:T(8,128)(2,1)S(1)} %collective-permute-done.3.refs_0_), channel_id=1, source_target_pairs={{32,0},{64,32},{96,64},{128,96},{160,128},{192,160},{224,192},{0,2... | collective-permute-start | bytes 786440 | tf_op jit(solution)/shard_map/ppermute | solution.py:33
  52.1 46.5 %collective-permute-start.6 = (bf16[512,256]{1,0:T(8,128)(2,1)S(1)}, bf16[512,256]{1,0:T(8,128)(2,1)S(1)}, u32[]{:S(2)}, u32[]{:S(2)}) collective-permute-start(bf16[512,256]{1,0:T(8,128)(2,1)S(1)} %collective-permute-done.4.refs_1_), channel_id=1, source_target_pairs={{224,0},{0,32},{32,64},{64,96},{96,128},{128,160},{160,192},{192,2... | collective-permute-start | bytes 786440 | tf_op jit(solution)/shard_map/ppermute | solution.py:33
  98.6 95.3 %collective-permute-start.11 = (bf16[64,2048]{1,0:T(8,128)(2,1)S(1)}, bf16[64,2048]{1,0:T(8,128)(2,1)S(1)}, u32[]{:S(2)}, u32[]{:S(2)}) collective-permute-start(bf16[64,2048]{1,0:T(8,128)(2,1)S(1)} %copy-done.1), channel_id=1, source_target_pairs={{1,0},{2,1},{3,2},{0,3},{5,4},{6,5},{7,6},{4,7},{9,8},{10,9},{11,1... | collective-permute-start | bytes 786440 | tf_op jit(solution)/shard_map/ppermute | solution.py:33
  98.7 95.2 %collective-permute-start.12 = (bf16[64,2048]{1,0:T(8,128)(2,1)S(1)}, bf16[64,2048]{1,0:T(8,128)(2,1)S(1)}, u32[]{:S(2)}, u32[]{:S(2)}) collective-permute-start(bf16[64,2048]{1,0:T(8,128)(2,1)S(1)} %copy-done.1), channel_id=1, source_target_pairs={{2,0},{3,1},{0,2},{1,3},{6,4},{7,5},{4,6},{5,7},{10,8},{11,9},{8,1... | collective-permute-start | bytes 786440 | tf_op jit(solution)/shard_map/ppermute | solution.py:33
  98.8 95.1 %collective-permute-start.13 = (bf16[64,2048]{1,0:T(8,128)(2,1)S(1)}, bf16[64,2048]{1,0:T(8,128)(2,1)S(1)}, u32[]{:S(2)}, u32[]{:S(2)}) collective-permute-start(bf16[64,2048]{1,0:T(8,128)(2,1)S(1)} %copy-done.1), channel_id=1, source_target_pairs={{3,0},{0,1},{1,2},{2,3},{7,4},{4,5},{5,6},{6,7},{11,8},{8,9},{9,10... | collective-permute-start | bytes 786440 | tf_op jit(solution)/shard_map/ppermute | solution.py:33
  100.7 46.5 %collective-permute-start.7 = (bf16[512,256]{1,0:T(8,128)(2,1)S(1)}, bf16[512,256]{1,0:T(8,128)(2,1)S(1)}, u32[]{:S(2)}, u32[]{:S(2)}) collective-permute-start(bf16[512,256]{1,0:T(8,128)(2,1)S(1)} %collective-permute-done.5.refs_0_), channel_id=1, source_target_pairs={{32,0},{64,32},{96,64},{128,96},{160,128},{192,160},{224,192},{0,2... | collective-permute-start | bytes 786440 | tf_op jit(solution)/shard_map/ppermute | solution.py:33
  100.7 46.5 %collective-permute-start.8 = (bf16[512,256]{1,0:T(8,128)(2,1)S(1)}, bf16[512,256]{1,0:T(8,128)(2,1)S(1)}, u32[]{:S(2)}, u32[]{:S(2)}) collective-permute-start(bf16[512,256]{1,0:T(8,128)(2,1)S(1)} %collective-permute-done.6.refs_1_), channel_id=1, source_target_pairs={{224,0},{0,32},{32,64},{64,96},{96,128},{128,160},{160,192},{192,2... | collective-permute-start | bytes 786440 | tf_op jit(solution)/shard_map/ppermute | solution.py:33
  147.2 46.7 %collective-permute-start.9 = (bf16[256,256]{1,0:T(8,128)(2,1)S(1)}, bf16[256,256]{1,0:T(8,128)(2,1)S(1)}, u32[]{:S(2)}, u32[]{:S(2)}) collective-permute-start(bf16[256,256]{1,0:T(8,128)(2,1)S(1)} %slice.6), channel_id=1, source_target_pairs={{32,0},{64,32},{96,64},{128,96},{160,128},{192,160},{224,192},{0,2... | collective-permute-start | bytes 393224 | tf_op jit(solution)/shard_map/ppermute | solution.py:33
  147.3 46.6 %collective-permute-start.10 = (bf16[256,256]{1,0:T(8,128)(2,1)S(1)}, bf16[256,256]{1,0:T(8,128)(2,1)S(1)}, u32[]{:S(2)}, u32[]{:S(2)}) collective-permute-start(bf16[256,256]{1,0:T(8,128)(2,1)S(1)} %slice.7), channel_id=1, source_target_pairs={{224,0},{0,32},{32,64},{64,96},{96,128},{128,160},{160,192},{192,2... | collective-permute-start | bytes 393224 | tf_op jit(solution)/shard_map/ppermute | solution.py:33
  217.7 2.8 %collective-permute-start.14 = (f32[8,136,256]{2,1,0:T(8,128)S(1)}, f32[8,136,256]{2,1,0:T(8,128)S(1)}, u32[]{:S(2)}, u32[]{:S(2)}) collective-permute-start(f32[8,136,256]{2,1,0:T(8,128)S(1)} %get-tuple-element.91), channel_id=1, source_target_pairs={{4,0},{0,4},{5,1},{1,5},{6,2},{2,6},{7,3},{3,7},{12,8},{8,12},{13,... | collective-permute-start | bytes 3342344 | tf_op jit(solution)/shard_map/ppermute | solution.py:33
  220.5 3.8 %copy-start.4 = (f32[2]{0:T(128)S(1)}, f32[2]{0:T(128)}, u32[]{:S(2)}) copy-start(f32[2]{0:T(128)} %lambdas.1) | copy-start | bytes 28
  220.6 9.6 %copy-start.5 = (f32[128]{0:T(128)S(1)}, f32[128]{0:T(128)}, u32[]{:S(2)}) copy-start(f32[128]{0:T(128)} %param.18) | copy-start | bytes 1540
  220.6 21.6 %copy-start.2 = (f32[2048]{0:T(1024)S(1)}, f32[2048]{0:T(1024)}, u32[]{:S(2)}) copy-start(f32[2048]{0:T(1024)} %param.20) | copy-start | bytes 24580
  220.6 21.5 %copy-start.3 = (f32[2048]{0:T(1024)S(1)}, f32[2048]{0:T(1024)}, u32[]{:S(2)}) copy-start(f32[2048]{0:T(1024)} %param.21) | copy-start | bytes 24580
  220.6 3.7 %collective-permute-start.15 = (f32[8,256]{1,0:T(8,128)S(1)}, f32[8,256]{1,0:T(8,128)S(1)}, u32[]{:S(2)}, u32[]{:S(2)}) collective-permute-start(f32[8,256]{1,0:T(8,128)S(1)} %levels.1), channel_id=1, source_target_pairs={{0,8},{8,0},{16,24},{24,16},{1,9},{9,1},{17,25},{25,17},{2,10},{10... | collective-permute-start | bytes 24584 | tf_op jit(solution)/shard_map/ppermute | solution.py:451
  225.1 5.1 %collective-permute-start.16 = (bf16[2,128,256]{2,1,0:T(8,128)(2,1)S(1)}, bf16[2,128,256]{2,1,0:T(8,128)(2,1)S(1)}, u32[]{:S(2)}, u32[]{:S(2)}) collective-permute-start(bf16[2,128,256]{2,1,0:T(8,128)(2,1)S(1)} %get-tuple-element.93), channel_id=1, source_target_pairs={{0,8},{8,0},{16,24},{24,16},{1,9},{9,1},{17,25},{25,17},{2,10},{10... | collective-permute-start | bytes 393224 | tf_op jit(solution)/shard_map/ppermute | solution.py:452
  230.4 8.3 %collective-permute-start.17 = (bf16[256,256]{1,0:T(8,128)(2,1)S(1)}, bf16[256,256]{1,0:T(8,128)(2,1)S(1)}, u32[]{:S(2)}, u32[]{:S(2)}) collective-permute-start(bf16[256,256]{1,0:T(8,128)(2,1)S(1)} %merge.1.h0), channel_id=1, source_target_pairs={{1,0},{2,1},{3,2},{0,3},{5,4},{6,5},{7,6},{4,7},{9,8},{10,9},{11,1... | collective-permute-start | bytes 393224 | tf_op jit(solution)/shard_map/ppermute | solution.py:33
  234.6 6.6 %collective-permute-start.18 = (bf16[256,256]{1,0:T(8,128)(2,1)S(1)}, bf16[256,256]{1,0:T(8,128)(2,1)S(1)}, u32[]{:S(2)}, u32[]{:S(2)}) collective-permute-start(bf16[256,256]{1,0:T(8,128)(2,1)S(1)} %merge.1.h0), channel_id=1, source_target_pairs={{2,0},{3,1},{0,2},{1,3},{6,4},{7,5},{4,6},{5,7},{10,8},{11,9},{8,1... | collective-permute-start | bytes 393224 | tf_op jit(solution)/shard_map/ppermute | solution.py:33
  234.6 7.6 %collective-permute-start.19 = (bf16[256,256]{1,0:T(8,128)(2,1)S(1)}, bf16[256,256]{1,0:T(8,128)(2,1)S(1)}, u32[]{:S(2)}, u32[]{:S(2)}) collective-permute-start(bf16[256,256]{1,0:T(8,128)(2,1)S(1)} %merge.1.h0), channel_id=1, source_target_pairs={{3,0},{0,1},{1,2},{2,3},{7,4},{4,5},{5,6},{6,7},{11,8},{8,9},{9,10... | collective-permute-start | bytes 393224 | tf_op jit(solution)/shard_map/ppermute | solution.py:33
  242.1 2.2 copy-start
  255.2 12.6 %copy-start.7 = (f32[2048]{0:T(1024)S(1)}, f32[2048]{0:T(1024)}, u32[]{:S(2)}) copy-start(f32[2048]{0:T(1024)} %param.22) | copy-start | bytes 24580
  255.2 9.7 %collective-permute-start.22 = (bf16[64,2048]{1,0:T(8,128)(2,1)S(1)}, bf16[64,2048]{1,0:T(8,128)(2,1)S(1)}, u32[]{:S(2)}, u32[]{:S(2)}) collective-permute-start(bf16[64,2048]{1,0:T(8,128)(2,1)S(1)} %get-tuple-element.104), channel_id=1, source_target_pairs={{2,0},{3,1},{0,2},{1,3},{6,4},{7,5},{4,6},{5,7},{10,8},{11,9},{8,1... | collective-permute-start | bytes 786440 | tf_op jit(solution)/shard_map/ppermute | solution.py:33
  256.2 9.9 %collective-permute-start.21 = (bf16[64,2048]{1,0:T(8,128)(2,1)S(1)}, bf16[64,2048]{1,0:T(8,128)(2,1)S(1)}, u32[]{:S(2)}, u32[]{:S(2)}) collective-permute-start(bf16[64,2048]{1,0:T(8,128)(2,1)S(1)} %get-tuple-element.103), channel_id=1, source_target_pairs={{1,0},{2,1},{3,2},{0,3},{5,4},{6,5},{7,6},{4,7},{9,8},{10,9},{11,1... | collective-permute-start | bytes 786440 | tf_op jit(solution)/shard_map/ppermute | solution.py:33
  257.0 10.6 %collective-permute-start.20 = (bf16[64,2048]{1,0:T(8,128)(2,1)S(1)}, bf16[64,2048]{1,0:T(8,128)(2,1)S(1)}, u32[]{:S(2)}, u32[]{:S(2)}) collective-permute-start(bf16[64,2048]{1,0:T(8,128)(2,1)S(1)} %get-tuple-element.102), channel_id=1, source_target_pairs={{3,0},{0,1},{1,2},{2,3},{7,4},{4,5},{5,6},{6,7},{11,8},{8,9},{9,10... | collective-permute-start | bytes 786440 | tf_op jit(solution)/shard_map/ppermute | solution.py:33
Sparse Core Ops, SparseCore 0:
  10.1 108.9 all-gather.1
